TPU v7x, 32 devices: a whole 2x2x4 slice. The times are simulated.
32 devices in a mesh: grp: 2 (over y), sp: 4 (over z), fs: 2 (over x), tp: 2 (over core).
Axes of the slice: x: 2, y: 2, z: 4, core: 2. Of those that a mesh axis runs over, the one named last changes fastest.
Arguments:
- tokens: bfloat16 [4, 1024, 2048], P(('grp', 'fs'), 'sp', 'tp'), parts along dimension 0, may hold values from -6 to 6
- input_norm_gain: float32 [2048], replicated, may hold values from 0.1 to 1.9
- query_weight: bfloat16 [2048, 1024], P('sp', 'tp'), may hold values from -0.125 to 0.125
- key_weight: bfloat16 [2048, 1024], P('sp', 'tp'), may hold values from -0.125 to 0.125
- value_weight: bfloat16 [2048, 1024], P('sp', 'tp'), may hold values from -0.125 to 0.125
- decay_gate_weight: bfloat16 [2048, 8], replicated, may hold values from -0.125 to 0.125
- write_strength_weight: bfloat16 [2048, 8], replicated, may hold values from -0.125 to 0.125
- up_weight: bfloat16 [2048, 1024], P('sp', 'tp'), may hold values from -0.125 to 0.125
- gate_half_weight: bfloat16 [2048, 1024], P('sp', 'tp'), may hold values from -0.125 to 0.125
- log_decay_rate: float32 [8], replicated, may hold values from -30 to 0
- write_strength_bias: float32 [8], replicated, may hold values from -7 to 1
- decay_spike_added: float32 [4, 1024, 8], P(('grp', 'fs'), 'sp', 'tp'), parts along dimension 0, may hold values from -2 to 0
- starting_state: float32 [4, 8, 128, 128], P(('grp', 'fs'), 'tp'), parts along dimension 0, may hold values from -4 to 4
- head_norm_gain: float32 [128], replicated, may hold values from 0.1 to 1.9
- convolution_kernel: float32 [31, 1024], replicated, may hold values from -4 to 4
- channel_norm_gain: float32 [1024], replicated, may hold values from 0.1 to 1.9
- delta_output_rows: bfloat16 [1024, 2048], P('tp', 'sp'), may hold values from -0.125 to 0.125
- convolution_output_rows: bfloat16 [1024, 2048], P('tp', 'sp'), may hold values from -0.125 to 0.125
Outputs:
- mixed: bfloat16 [4, 1024, 2048], P(('grp', 'fs'), 'sp', 'tp'), parts along dimension 0
There are 2 independent parts, one for each index of `grp`. A program takes and returns all parts, laid end to end along the dimension named above; an argument that names none is the same for every part. Nothing has to cross between parts.
All inputs are finite; a program needn't handle non-finite values.
Results may differ from a plain program's by a relative error of at most 0.01.
Values may be sent and summed in bfloat16 or wider, within the bound.
A program may use at most 64 MiB of HBM per device.

v0:
```python
import jax
import jax.numpy as jnp
from jax import lax
from jax.sharding import PartitionSpec as P

HEADS = 8
HEAD = 128
CH = 1024
KSIZE = 31
BLOCK = 64


EPS = 1e-06
HIGH = lax.Precision.HIGHEST


def from_behind(block, axis, distance):
    devices = range(lax.axis_size(axis))
    route = [(i - distance, i) for i in devices if i - distance in devices]
    return lax.ppermute(block, axis, route)


def unit_rows(values):
    return values * lax.rsqrt(jnp.sum(values * values, axis=-1, keepdims=True) + EPS)


def rounded(values):
    return lax.optimization_barrier(values.astype(jnp.bfloat16)).astype(jnp.float32)


def block_terms(query, keys, values, log_decay, beta, blen):
    rows = keys.shape[0]
    count = rows // blen

    def split_blocks(array):
        return jnp.swapaxes(array.reshape((count, blen) + array.shape[1:]), 1, 2)

    q_blocks, k_blocks, v_blocks = (split_blocks(query), split_blocks(keys), split_blocks(values))
    g_blocks, b_blocks = (split_blocks(log_decay), split_blocks(beta))
    cumdec = jnp.cumsum(g_blocks, axis=-1)
    lower = jnp.tril(jnp.ones((blen, blen), bool))
    strict = jnp.tril(jnp.ones((blen, blen), bool), -1)
    diff = cumdec[..., :, None] - cumdec[..., None, :]
    gamma = jnp.where(lower, jnp.exp(jnp.where(lower, diff, 0.0)), 0.0)
    k_beta = k_blocks * b_blocks[..., None]
    a_matrix = jnp.where(
        strict, jnp.einsum("nhid,nhjd->nhij", k_beta, k_blocks, precision=HIGH) * gamma, 0.0
    )
    left_side = a_matrix + jnp.eye(blen, dtype=jnp.float32)
    right_side = jnp.concatenate(
        [v_blocks * b_blocks[..., None], k_beta * jnp.exp(cumdec)[..., None]], axis=-1
    )
    solved = jax.scipy.linalg.solve_triangular(
        left_side, right_side, lower=True, unit_diagonal=True
    )
    width_v = v_blocks.shape[-1]
    updates, w_rows = (solved[..., :width_v], solved[..., width_v:])
    q_k = jnp.where(
        lower, jnp.einsum("nhid,nhjd->nhij", q_blocks, k_blocks, precision=HIGH) * gamma, 0.0
    )
    last = cumdec[..., -1]
    k_decayed = k_blocks * jnp.exp(last[..., None] - cumdec)[..., None]
    q_decayed = q_blocks * jnp.exp(cumdec)[..., None]
    return (q_decayed, k_decayed, updates, w_rows, q_k, last)


def device_map(terms, width_k, width_v, heads):
    q_decayed, k_decayed, updates, w_rows, q_k, last = terms
    identity = jnp.broadcast_to(jnp.eye(width_k, dtype=jnp.float32), (heads, width_k, width_k))

    def compose(carry, input_rows):
        maps, offsets = carry
        k_part, u_part, w_part, last_part = input_rows
        step_map = jnp.exp(last_part)[:, None, None] * identity - jnp.einsum(
            "hcd,hce->hde", k_part, w_part, precision=HIGH
        )
        maps = jnp.einsum("hde,hef->hdf", step_map, maps, precision=HIGH)
        offsets = jnp.einsum("hde,hef->hdf", step_map, offsets, precision=HIGH) + jnp.einsum(
            "hcd,hce->hde", k_part, u_part, precision=HIGH
        )
        return ((maps, offsets), None)

    start = (identity, jnp.zeros((heads, width_k, width_v), jnp.float32))
    (maps, offsets), _ = lax.scan(compose, start, (k_decayed, updates, w_rows, last))
    return (maps, offsets, identity)


def block_outputs(start_state, terms):

    def advance(state, input_rows):
        q_decayed, k_decayed, updates, w_rows, q_k, last = input_rows
        v_new = updates - jnp.einsum("hcd,hde->hce", w_rows, state, precision=HIGH)
        output = jnp.einsum("hcd,hde->hce", q_decayed, state, precision=HIGH) + jnp.einsum(
            "hij,hje->hie", q_k, v_new, precision=HIGH
        )
        state = state * jnp.exp(last)[..., None, None] + jnp.einsum(
            "hcd,hce->hde", k_decayed, v_new, precision=HIGH
        )
        return (state, output)

    _, outputs = lax.scan(advance, start_state, terms)
    count, heads, blen, width_v = outputs.shape
    return jnp.swapaxes(outputs, 1, 2).reshape(count * blen, heads, width_v)


def apply_map(maps, state):
    return jnp.einsum("hde,hef->hdf", maps, state, precision=HIGH)


def on_device(
    tokens,
    input_norm_gain,
    query_weight,
    key_weight,
    value_weight,
    decay_gate_weight,
    write_strength_weight,
    up_weight,
    gate_half_weight,
    log_decay_rate,
    write_strength_bias,
    decay_spike_added,
    starting_state,
    head_norm_gain,
    convolution_kernel,
    channel_norm_gain,
    delta_output_rows,
    convolution_output_rows,
):
    rows = tokens.shape[1]
    heads_here = query_weight.shape[1] // HEAD
    chan_here = up_weight.shape[1]
    tp_index = lax.axis_index("tp")
    sp_index = lax.axis_index("sp")
    gathered = lax.all_gather(tokens[0], "tp", axis=1, tiled=True)
    token_f = gathered.astype(jnp.float32)
    normed = (
        token_f
        * lax.rsqrt(jnp.mean(token_f * token_f, axis=-1, keepdims=True) + EPS)
        * input_norm_gain
    ).astype(jnp.bfloat16)
    pieces = (
        lax.all_gather(query_weight, "sp", axis=0, tiled=True),
        lax.all_gather(key_weight, "sp", axis=0, tiled=True),
        lax.all_gather(value_weight, "sp", axis=0, tiled=True),
        lax.all_gather(up_weight, "sp", axis=0, tiled=True),
        lax.all_gather(gate_half_weight, "sp", axis=0, tiled=True),
    )
    q_sum, k_sum, v_sum, up_sum, gate_sum = tuple(
        (jnp.dot(normed, piece, preferred_element_type=jnp.float32) for piece in pieces)
    )
    glu = lax.optimization_barrier(
        (rounded(up_sum) * jax.nn.sigmoid(rounded(gate_sum))).astype(jnp.bfloat16)
    )
    rim = from_behind(glu[rows - (KSIZE - 1) :], "sp", 1)
    shape = (rows, heads_here, HEAD)
    query = unit_rows(jax.nn.silu(rounded(q_sum)).reshape(shape)) * HEAD ** (-0.5)
    keys = unit_rows(jax.nn.silu(rounded(k_sum)).reshape(shape))
    values = jax.nn.silu(rounded(v_sum)).reshape(shape)
    gate_cols = jnp.concatenate([decay_gate_weight, write_strength_weight], axis=1)
    small_raw = rounded(jnp.dot(normed, gate_cols, preferred_element_type=jnp.float32))
    head_start = tp_index * heads_here
    decay_logits = lax.dynamic_slice_in_dim(small_raw[:, :HEADS], head_start, heads_here, 1)
    beta_raw = lax.dynamic_slice_in_dim(small_raw[:, HEADS:], head_start, heads_here, 1)
    decay_rates = jnp.exp(lax.dynamic_slice_in_dim(log_decay_rate, head_start, heads_here, 0))
    bias_here = lax.dynamic_slice_in_dim(write_strength_bias, head_start, heads_here, 0)
    log_decay = -decay_rates * jax.nn.softplus(decay_logits) + decay_spike_added[0]
    beta = jax.nn.sigmoid(beta_raw + bias_here)
    terms = block_terms(query, keys, values, log_decay, beta, BLOCK)
    maps, offsets, identity = device_map(terms, HEAD, HEAD, heads_here)
    start_state = starting_state[0]
    first = sp_index == 0

    def relay(turn, incoming):
        outgoing = apply_map(maps, incoming) + offsets
        arrived = from_behind(outgoing, "sp", 1)
        return jnp.where(first, start_state, arrived)

    state_in = lax.fori_loop(
        0,
        lax.axis_size("sp") - 1,
        relay,
        jnp.where(first, start_state, jnp.zeros_like(start_state)),
    )
    extended = jnp.concatenate([rim, glu], axis=0).astype(jnp.float32)
    taps_here = lax.dynamic_slice_in_dim(convolution_kernel, tp_index * chan_here, chan_here, 1)
    conv = jnp.zeros((rows, chan_here), jnp.float32)
    for tap in range(KSIZE):
        conv = conv + taps_here[tap] * extended[tap : tap + rows]
    row_sum, row_squares = lax.psum((jnp.sum(conv, axis=-1), jnp.sum(conv * conv, axis=-1)), "tp")
    mean_c = (row_sum / CH)[:, None]
    var_c = (row_squares / CH)[:, None] - mean_c * mean_c
    gain_here = lax.dynamic_slice_in_dim(channel_norm_gain, tp_index * chan_here, chan_here, 0)
    conv_out = jax.nn.silu((conv - mean_c) * lax.rsqrt(var_c + EPS) * gain_here).astype(
        jnp.bfloat16
    )
    attn = block_outputs(state_in, terms)
    attn_out = (
        attn * lax.rsqrt(jnp.mean(attn * attn, axis=-1, keepdims=True) + EPS) * head_norm_gain
    ).astype(jnp.bfloat16)
    attn_out = attn_out.reshape(rows, heads_here * HEAD)
    pieces = (
        lax.all_gather(delta_output_rows, "sp", axis=1, tiled=True),
        lax.all_gather(convolution_output_rows, "sp", axis=1, tiled=True),
    )
    term = jnp.dot(attn_out, pieces[0], preferred_element_type=jnp.float32) + jnp.dot(
        conv_out, pieces[1], preferred_element_type=jnp.float32
    )
    mixed = lax.psum_scatter(term.astype(jnp.bfloat16), "tp", scatter_dimension=1, tiled=True)
    return mixed[None]


def solution(mesh):
    return jax.shard_map(
        on_device,
        mesh=mesh,
        in_specs=(
            P(("grp", "fs"), "sp", "tp"),
            P(),
            P("sp", "tp"),
            P("sp", "tp"),
            P("sp", "tp"),
            P(),
            P(),
            P("sp", "tp"),
            P("sp", "tp"),
            P(),
            P(),
            P(("grp", "fs"), "sp", "tp"),
            P(("grp", "fs"), "tp", None, None),
            P(),
            P(),
            P(),
            P("tp", "sp"),
            P("tp", "sp"),
        ),
        out_specs=P(("grp", "fs"), "sp", "tp"),
        check_vma=False,
    )
```

profile of v0, /device:TPU:0, one launch (start us, length us, event | category | flops | bytes accessed | tf_op | source)
XLA Modules:
  0.0 376.2 jit_solution(2804869446033036344)
XLA Ops:
  6.5 0.7 all-gather.24.cloned.1.call-update
  10.6 0.7 all-gather.16.cloned.1.call-update
  11.3 0.7 all-gather.22.cloned.1.call-update
  14.3 1.8 fusion.133
  16.1 2.0 constant_dynamic-slice_fusion.2
  18.1 2.6 all-gather.24.cloned.1.call-done
  20.7 1.6 fusion.37
  22.3 1.7 convolution_convert_fusion.5
  24.2 1.0 reduce_window_sum.11
  25.5 43.6 %all-gather.10.cloned.1.call-done = bf16[2048,512]{1,0:T(8,128)(2,1)} async-done(((bf16[512,512]{1,0:T(8,128)(2,1)}), bf16[2048,512]{1,0:T(8,128)(2,1)}) %all-gather.10.cloned.1.call-update) | async-done | bytes 2097168 | tf_op jit(solution)/shard_map/all_gather | solution.py:144
  69.1 2.4 convolution_convert_fusion.4
  72.5 42.6 %all-gather.14.cloned.1.call-done = bf16[2048,512]{1,0:T(8,128)(2,1)} async-done(((bf16[512,512]{1,0:T(8,128)(2,1)}), bf16[2048,512]{1,0:T(8,128)(2,1)}) %all-gather.14.cloned.1.call-update) | async-done | bytes 2097168 | tf_op jit(solution)/shard_map/all_gather | solution.py:143
  115.2 2.4 convolution_convert_fusion.2
  118.7 42.4 %all-gather.12.cloned.1.call-done = bf16[2048,512]{1,0:T(8,128)(2,1)} async-done(((bf16[512,512]{1,0:T(8,128)(2,1)}), bf16[2048,512]{1,0:T(8,128)(2,1)}) %all-gather.12.cloned.1.call-update) | async-done | bytes 2097168 | tf_op jit(solution)/shard_map/all_gather | solution.py:145
  161.1 2.7 convolution_convert_fusion.3
  164.2 1.3 fusion.45
  165.5 78.6 %custom-call.4 = f32[4,4,1,64,64]{3,4,2,1,0:T(8,128)S(1)} custom-call(f32[4,4,1,64,64]{4,3,2,1,0:T(8,128)S(1)} %fusion.45), custom_call_target="InvertDiagBlocksLowerTriangular" | custom-call | tf_op jit(solution)/shard_map/jit(_solve_triangular)/vmap(vmap())/triangular_solve | solution.py:53
  244.1 2.7 fusion.40
  246.8 1.5 multiply_multiply_fusion
  248.3 1.1 fusion.46
  249.6 8.4 %while.37 = (s32[]{:T(128)}, f32[4,128,128]{2,1,0:T(8,128)S(1)}, f32[4,128,128]{2,1,0:T(8,128)S(1)}, f32[4,4]{1,0:T(4,128)S(1)}, f32[4,4,64,128]{3,2,1,0:T(8,128...) while((s32[]{:T(128)}, f32[4,128,128]{2,1,0:T(8,128)S(1)}, ...), condition=%wide.region_4.5_spmd.clone, body=%wide.region_3.4_spmd.clone.sunk | while | flops 302252032 | bytes 3476115 | solution.py:84
  258.0 51.4 %while.35 = (s32[]{:T(128)}, f32[4,128,128]{2,1,0:T(8,128)S(1)}, pred[]{:T(512)}, f32[4,128,128]{2,1,0:T(8,128)S(1)}, f32[4,128,128]{2,1,0:T(8,128)S(1)}, /*index=5*/f32[4,128,128]{2,1,0:T(8,128)S(1)}, s32[]{:T(128)}) while((s32[]{:T(128)}, f32[4,128,128]{2,1,0:T(8,128)S(1)}, pred[]{:T(512)}, f32[4,128,128]{2,1,0:T(8,128)S(1)}, ...), condition=%wide.region_6.7_spmd, body=%wide.region_5.6_spmd.sunk | while | flops 100794368 | bytes 2883702 | solution.py:179
  258.4 2.1 collective-permute-start
  260.5 9.1 %collective-permute-done = f32[4,128,128]{2,1,0:T(8,128)S(1)} collective-permute-done((f32[4,128,128]{2,1,0:T(8,128)S(1)}, f32[4,128,128]{2,1,0:T(8,128)S(1)}, u32[]{:S(2)}, u32[]{:S(2)}) %collective-permute-start) | collective-permute-done | bytes 262176 | tf_op jit(solution)/shard_map/while/body/eval_jaxpr/ppermute | solution.py:20
  270.0 8.4 %collective-permute-start = (f32[4,128,128]{2,1,0:T(8,128)S(1)}, f32[4,128,128]{2,1,0:T(8,128)S(1)}, u32[]{:S(2)}, u32[]{:S(2)}) collective-permute-start(f32[4,128,128]{2,1,0:T(8,128)S(1)} %convolution_add_fusion.8), channel_id=1, source_target_pairs={{0,4},{4,8},{8,12},{1,5},{5,9},{9,13},{2,6},{6,10},{10,14},{3,7},{... | collective-permute-start | bytes 786440 | tf_op jit(solution)/shard_map/while/body/eval_jaxpr/ppermute | solution.py:20
  278.4 9.7 %collective-permute-done = f32[4,128,128]{2,1,0:T(8,128)S(1)} collective-permute-done((f32[4,128,128]{2,1,0:T(8,128)S(1)}, f32[4,128,128]{2,1,0:T(8,128)S(1)}, u32[]{:S(2)}, u32[]{:S(2)}) %collective-permute-start) | collective-permute-done | bytes 262176 | tf_op jit(solution)/shard_map/while/body/eval_jaxpr/ppermute | solution.py:20
  288.6 11.1 %collective-permute-start = (f32[4,128,128]{2,1,0:T(8,128)S(1)}, f32[4,128,128]{2,1,0:T(8,128)S(1)}, u32[]{:S(2)}, u32[]{:S(2)}) collective-permute-start(f32[4,128,128]{2,1,0:T(8,128)S(1)} %convolution_add_fusion.8), channel_id=1, source_target_pairs={{0,4},{4,8},{8,12},{1,5},{5,9},{9,13},{2,6},{6,10},{10,14},{3,7},{... | collective-permute-start | bytes 786440 | tf_op jit(solution)/shard_map/while/body/eval_jaxpr/ppermute | solution.py:20
  299.7 9.6 %collective-permute-done = f32[4,128,128]{2,1,0:T(8,128)S(1)} collective-permute-done((f32[4,128,128]{2,1,0:T(8,128)S(1)}, f32[4,128,128]{2,1,0:T(8,128)S(1)}, u32[]{:S(2)}, u32[]{:S(2)}) %collective-permute-start) | collective-permute-done | bytes 262176 | tf_op jit(solution)/shard_map/while/body/eval_jaxpr/ppermute | solution.py:20
  309.4 16.7 %while.36 = (s32[]{:T(128)}, f32[4,128,128]{2,1,0:T(8,128)S(1)}, f32[4,4,64,128]{3,2,1,0:T(8,128)}, f32[4,4]{1,0:T(4,128)S(1)}, f32[4,4,64,128]{3,2,1,0:T(8,128)...) while((s32[]{:T(128)}, f32[4,128,128]{2,1,0:T(8,128)S(1)}, ...), condition=%wide.region_9.10_spmd, body=%wide.region_8.9_spmd.sunk | while | flops 176357376 | bytes 2493581 | solution.py:101
  309.9 1.2 fusion.188
  311.1 1.9 fusion.189
  314.1 1.2 fusion.188
  315.2 1.9 fusion.189
  318.2 1.2 fusion.188
  319.4 1.9 fusion.189
  322.3 1.2 fusion.188
  323.5 1.9 fusion.189
  326.1 1.3 multiply_reduce_fusion.1
  327.5 1.4 copy.68
  328.9 2.7 convolution_convert_fusion.1
  331.7 2.4 convolution_convert_fusion
  334.3 5.0 %collective-permute-start.1 = (bf16[30,512]{1,0:T(8,128)(2,1)S(1)}, bf16[30,512]{1,0:T(8,128)(2,1)S(1)}, u32[]{:S(2)}, u32[]{:S(2)}) collective-permute-start(bf16[30,512]{1,0:T(8,128)(2,1)S(1)} %slice.283), channel_id=1, source_target_pairs={{0,4},{4,8},{8,12},{1,5},{5,9},{9,13},{2,6},{6,10},{10,14},{3,7},{... | collective-permute-start | bytes 92168 | tf_op jit(solution)/shard_map/ppermute | solution.py:20
  339.9 2.3 fusion.98
  342.6 2.7 fusion.130
  345.3 2.5 all-reduce
  347.8 10.5 %all-gather.22.cloned.1.call-done = bf16[512,2048]{1,0:T(8,128)(2,1)} async-done(((bf16[512,512]{1,0:T(8,128)(2,1)}), bf16[512,2048]{1,0:T(8,128)(2,1)}) %all-gather.22.cloned.1.call-update) | async-done | bytes 2097168 | tf_op jit(solution)/shard_map/all_gather | solution.py:204
  358.2 3.5 fusion.36
  361.7 8.0 %reduce-scatter.2.cloned.1.call-done = bf16[256,1024]{1,0:T(8,128)(2,1)} async-done(((bf16[256,2048]{1,0:T(8,128)(2,1)}), bf16[256,1024]{1,0:T(8,128)(2,1)}) %reduce-scatter.2.cloned.1.call-update) | async-done | bytes 524304 | tf_op jit(solution)/shard_map/reduce_scatter | solution.py:209
  (202 shorter events, 22.8 us)
Async XLA Ops:
  6.5 7.1 %copy-start = (f32[128]{0:T(128)S(1)}, f32[128]{0:T(128)}, u32[]{:S(2)}) copy-start(f32[128]{0:T(128)} %param.37) | copy-start | bytes 1540
  6.5 6.2 %copy-start.47 = (f32[8]{0:T(128)S(1)}, f32[8]{0:T(128)}, u32[]{:S(2)}) copy-start(f32[8]{0:T(128)} %param.34) | copy-start | bytes 100
  6.5 6.3 %copy-start.48 = (f32[8]{0:T(128)S(1)}, f32[8]{0:T(128)}, u32[]{:S(2)}) copy-start(f32[8]{0:T(128)} %param.33) | copy-start | bytes 100
  6.5 14.1 %all-gather.24.cloned.1.call-start = ((), (), s32[]{:S(2)}) async-start(), calls=%async_computation.9 | async-start | bytes 1572864 | tf_op jit(solution)/shard_map/all_gather | solution.py:135
  7.3 6.4 %copy-start.1 = (f32[1,4,128,128]{3,2,1,0:T(8,128)S(1)}, f32[1,4,128,128]{3,2,1,0:T(8,128)}, u32[]{:S(2)}) copy-start(f32[1,4,128,128]{3,2,1,0:T(8,128)} %param.36) | copy-start | bytes 786436
  7.3 61.8 %all-gather.10.cloned.1.call-start = ((), (), s32[]{:S(2)}) async-start(), calls=%async_computation.1 | async-start | bytes 2621440 | tf_op jit(solution)/shard_map/all_gather | solution.py:144
  8.0 5.6 %copy-start.37 = (f32[1024]{0:T(1024)S(1)}, f32[1024]{0:T(1024)}, u32[]{:S(2)}) copy-start(f32[1024]{0:T(1024)} %param.39) | copy-start | bytes 12292
  8.0 107.1 %all-gather.14.cloned.1.call-start = ((), (), s32[]{:S(2)}) async-start(), calls=%async_computation.3 | async-start | bytes 2621440 | tf_op jit(solution)/shard_map/all_gather | solution.py:143
  8.8 152.3 %all-gather.12.cloned.1.call-start = ((), (), s32[]{:S(2)}) async-start(), calls=%async_computation.2 | async-start | bytes 2621440 | tf_op jit(solution)/shard_map/all_gather | solution.py:145
  9.3 12.9 %copy-start.42 = (bf16[2048,8]{0,1:T(8,128)(2,1)S(1)}, bf16[2048,8]{0,1:T(8,128)(2,1)}, u32[]{:S(2)}) copy-start(bf16[2048,8]{0,1:T(8,128)(2,1)} %param.30) | copy-start | bytes 98308
  9.4 12.9 %copy-start.43 = (bf16[2048,8]{0,1:T(8,128)(2,1)S(1)}, bf16[2048,8]{0,1:T(8,128)(2,1)}, u32[]{:S(2)}) copy-start(bf16[2048,8]{0,1:T(8,128)(2,1)} %param.29) | copy-start | bytes 98308
  9.4 12.9 %copy-start.44 = (f32[2048]{0:T(1024)S(1)}, f32[2048]{0:T(1024)}, u32[]{:S(2)}) copy-start(f32[2048]{0:T(1024)} %param.25) | copy-start | bytes 24580
  9.4 319.5 %all-gather.18.cloned.1.call-start = ((), (), s32[]{:S(2)}) async-start(), calls=%async_computation.5 | async-start | bytes 2621440 | tf_op jit(solution)/shard_map/all_gather | solution.py:146
  10.0 321.7 %all-gather.20.cloned.1.call-start = ((), (), s32[]{:S(2)}) async-start(), calls=%async_computation.6 | async-start | bytes 2621440 | tf_op jit(solution)/shard_map/all_gather | solution.py:147
  10.5 328.8 %all-gather.16.cloned.1.call-start = ((), (), s32[]{:S(2)}) async-start(), calls=%async_computation.4 | async-start | bytes 2621440 | tf_op jit(solution)/shard_map/all_gather | solution.py:203
  11.3 346.9 %all-gather.22.cloned.1.call-start = ((), (), s32[]{:S(2)}) async-start(), calls=%async_computation.7 | async-start | bytes 2621440 | tf_op jit(solution)/shard_map/all_gather | solution.py:204
  12.0 12.0 %copy-start.35 = (f32[1,256,4]{1,2,0:T(4,128)S(1)}, f32[1,256,4]{1,2,0:T(4,128)}, u32[]{:S(2)}) copy-start(f32[1,256,4]{1,2,0:T(4,128)} %param.35) | copy-start | bytes 12292
  12.0 357.6 %reduce-scatter.2.cloned.1.call-start = ((), (), s32[]{:S(2)}) async-start(), calls=%async_computation.8 | async-start | bytes 1572864 | tf_op jit(solution)/shard_map/reduce_scatter | solution.py:209
  20.7 48.4 %copy-start.2 = (bf16[1,256,2048]{2,1,0:T(8,128)(2,1)S(1)}, bf16[1,256,2048]{2,1,0:T(8,128)(2,1)}, u32[]{:S(2)}) copy-start(bf16[1,256,2048]{2,1,0:T(8,128)(2,1)} %all-gather.24.cloned.1.call-done) | copy-start | bytes 3145732
  22.3 46.8 %copy-start.38 = (f32[256]{0:T(256)}, f32[256]{0:T(256)S(1)}, u32[]{:S(2)}) copy-start(f32[256]{0:T(256)S(1)} %add_rsqrt_fusion.4) | copy-start | bytes 3076
  25.3 46.2 %copy-start.33 = (f32[4,4]{1,0:T(4,128)}, f32[4,4]{1,0:T(4,128)S(1)}, u32[]{:S(2)}) copy-start(f32[4,4]{1,0:T(4,128)S(1)} %slice_reduce_fusion) | copy-start | bytes 196
  71.5 43.7 %copy-start.39 = (f32[256]{0:T(256)S(1)}, f32[256]{0:T(256)}, u32[]{:S(2)}) copy-start(f32[256]{0:T(256)} %copy-done.38) | copy-start | bytes 3076
  117.6 43.5 %copy-start.40 = (f32[256]{0:T(256)S(1)}, f32[256]{0:T(256)}, u32[]{:S(2)}) copy-start(f32[256]{0:T(256)} %copy-done.38) | copy-start | bytes 3076
  117.6 43.5 %copy-start.45 = (f32[2048]{0:T(1024)S(1)}, f32[2048]{0:T(1024)}, u32[]{:S(2)}) copy-start(f32[2048]{0:T(1024)} %param.25) | copy-start | bytes 24580
  118.6 45.5 %copy-start.4 = (f32[64,64]{1,0:T(8,128)S(1)}, f32[64,64]{1,0:T(8,128)}, u32[]{:S(2)}) copy-start(f32[64,64]{1,0:T(8,128)} %get-tuple-element.263) | copy-start | bytes 49156
  118.7 45.5 %copy-start.5 = (f32[64,64]{1,0:T(8,128)S(1)}, f32[64,64]{1,0:T(8,128)}, u32[]{:S(2)}) copy-start(f32[64,64]{1,0:T(8,128)} %get-tuple-element.264) | copy-start | bytes 49156
  118.7 45.5 %copy-start.31 = (pred[64,64]{1,0:T(8,128)(4,1)S(1)}, pred[64,64]{1,0:T(8,128)(4,1)}, u32[]{:S(2)}) copy-start(pred[64,64]{1,0:T(8,128)(4,1)} %get-tuple-element.261) | copy-start | bytes 12292
  118.7 45.5 %copy-start.32 = (pred[64,64]{1,0:T(8,128)(4,1)S(1)}, pred[64,64]{1,0:T(8,128)(4,1)}, u32[]{:S(2)}) copy-start(pred[64,64]{1,0:T(8,128)(4,1)} %get-tuple-element.262) | copy-start | bytes 12292
  258.4 11.2 %collective-permute-start = (f32[4,128,128]{2,1,0:T(8,128)S(1)}, f32[4,128,128]{2,1,0:T(8,128)S(1)}, u32[]{:S(2)}, u32[]{:S(2)}) collective-permute-start(f32[4,128,128]{2,1,0:T(8,128)S(1)} %convolution_add_fusion.8), channel_id=1, source_target_pairs={{0,4},{4,8},{8,12},{1,5},{5,9},{9,13},{2,6},{6,10},{10,14},{3,7},{... | collective-permute-start | bytes 786440 | tf_op jit(solution)/shard_map/while/body/eval_jaxpr/ppermute | solution.py:20
  270.0 18.1 %collective-permute-start = (f32[4,128,128]{2,1,0:T(8,128)S(1)}, f32[4,128,128]{2,1,0:T(8,128)S(1)}, u32[]{:S(2)}, u32[]{:S(2)}) collective-permute-start(f32[4,128,128]{2,1,0:T(8,128)S(1)} %convolution_add_fusion.8), channel_id=1, source_target_pairs={{0,4},{4,8},{8,12},{1,5},{5,9},{9,13},{2,6},{6,10},{10,14},{3,7},{... | collective-permute-start | bytes 786440 | tf_op jit(solution)/shard_map/while/body/eval_jaxpr/ppermute | solution.py:20
  288.6 20.8 %collective-permute-start = (f32[4,128,128]{2,1,0:T(8,128)S(1)}, f32[4,128,128]{2,1,0:T(8,128)S(1)}, u32[]{:S(2)}, u32[]{:S(2)}) collective-permute-start(f32[4,128,128]{2,1,0:T(8,128)S(1)} %convolution_add_fusion.8), channel_id=1, source_target_pairs={{0,4},{4,8},{8,12},{1,5},{5,9},{9,13},{2,6},{6,10},{10,14},{3,7},{... | collective-permute-start | bytes 786440 | tf_op jit(solution)/shard_map/while/body/eval_jaxpr/ppermute | solution.py:20
  309.3 19.6 %copy-start.41 = (f32[256]{0:T(256)S(1)}, f32[256]{0:T(256)}, u32[]{:S(2)}) copy-start(f32[256]{0:T(256)} %copy-done.38) | copy-start | bytes 3076
  309.4 19.6 %copy-start.46 = (f32[2048]{0:T(1024)S(1)}, f32[2048]{0:T(1024)}, u32[]{:S(2)}) copy-start(f32[2048]{0:T(1024)} %param.25) | copy-start | bytes 24580
  328.9 2.8 copy-start.3
  334.3 8.0 %collective-permute-start.1 = (bf16[30,512]{1,0:T(8,128)(2,1)S(1)}, bf16[30,512]{1,0:T(8,128)(2,1)S(1)}, u32[]{:S(2)}, u32[]{:S(2)}) collective-permute-start(bf16[30,512]{1,0:T(8,128)(2,1)S(1)} %slice.283), channel_id=1, source_target_pairs={{0,4},{4,8},{8,12},{1,5},{5,9},{9,13},{2,6},{6,10},{10,14},{3,7},{... | collective-permute-start | bytes 92168 | tf_op jit(solution)/shard_map/ppermute | solution.py:20
  339.6 2.7 copy-start.6
  339.7 2.7 copy-start.7
  339.7 2.7 copy-start.8
  339.7 2.7 copy-start.9
  339.7 2.7 copy-start.10
  339.7 2.7 copy-start.11
  339.7 2.7 copy-start.12
  339.7 2.7 copy-start.13
  339.7 2.7 copy-start.14
  339.7 2.7 copy-start.15
  339.7 2.7 copy-start.16
  339.8 2.7 copy-start.17
  342.6 15.6 %copy-start.36 = (f32[512]{0:T(512)S(1)}, f32[512]{0:T(512)}, u32[]{:S(2)}) copy-start(f32[512]{0:T(512)} %dynamic_slice.56) | copy-start | bytes 6148
  (14 other events, 36.1 us)
Sparse Core Ops, SparseCore 0:
  8.9 11.7 all-gather.23
  22.2 46.8 all-gather.9
  70.7 44.4 all-gather.13
  116.6 44.4 all-gather.11
  162.5 44.8 all-gather.17
  208.9 45.2 all-gather.19
  255.7 54.8 all-gather.15
  312.2 46.0 all-gather.21
  361.8 7.7 reduce-scatter.1
where the time goes:
time: 377 us; the launch traced here: 376 us
  waiting for transfers between devices  183 us (49%)
  other arithmetic  89.8 us (24%)
  matrix products  50.6 us (13%)
  starting transfers between devices  26.9 us (7%)
  between operations  14.2 us (4%)
  local copies, waits for them, and re-layouts  8.34 us (2%)
    another operation x2, other arithmetic, block_terms(): jax.scipy.linalg.solve_triangular(left_side, right_side, lower=True, unit...  78.6 us
    all_gather x1, waiting for transfers between devices, on_device(): lax.all_gather(key_weight, 'sp', axis=0, tiled=True)  43.6 us
    all_gather x1, waiting for transfers between devices, on_device(): lax.all_gather(query_weight, 'sp', axis=0, tiled=True)  42.6 us
    all_gather x1, waiting for transfers between devices, on_device(): lax.all_gather(value_weight, 'sp', axis=0, tiled=True)  42.4 us
    ppermute x4, waiting for transfers between devices, from_behind(): return lax.ppermute(block, axis, route)  28.4 us
    ppermute x4, starting transfers between devices, from_behind(): return lax.ppermute(block, axis, route)  26.6 us
    dot_general x5, matrix products, on_device(): jnp.dot(normed, piece, preferred_element_type=jnp.float32)  12.5 us
    all_gather x1, waiting for transfers between devices, on_device(): lax.all_gather(convolution_output_rows, 'sp', axis=1, tiled=True)  10.5 us
  transfers between devices with their start and end apart: 13, of which 9 were waited for; matrix products, arithmetic and copies ran while one was open for 39% of the time, Pallas kernels for 0%

commit v1 on v0

v1 whole, which is shorter than its diff:
```python
import functools

import jax
import jax.numpy as jnp
from jax import lax
from jax.experimental import pallas as pl
from jax.experimental.pallas import tpu as pltpu
from jax.sharding import PartitionSpec as P

HEAD = 128
EPS = 1e-06
HIGH = lax.Precision.HIGHEST


def from_behind(block, axis, distance):
    devices = range(lax.axis_size(axis))
    route = [(i - distance, i) for i in devices if i - distance in devices]
    return lax.ppermute(block, axis, route)


def rounded(values):
    return lax.optimization_barrier(values.astype(jnp.bfloat16)).astype(jnp.float32)


def mm(a, b, precision=None):
    return jnp.dot(a, b, preferred_element_type=jnp.float32, precision=precision)


def mm_nt(a, b, precision=None):
    return lax.dot_general(
        a, b, (((1,), (1,)), ((), ())), preferred_element_type=jnp.float32, precision=precision
    )


def mm_tn(a, b, precision=None):
    return lax.dot_general(
        a, b, (((0,), (0,)), ((), ())), preferred_element_type=jnp.float32, precision=precision
    )


def silu(x):
    return x * jax.nn.sigmoid(x)


def unit(x):
    return x * lax.rsqrt(jnp.sum(x * x, axis=-1, keepdims=True) + EPS)


def delta_kernel(q_ref, k_ref, v_ref, cum_col_ref, cum_row_ref, beta_ref, p_ref, u_ref, m_ref, o_ref):
    units, rows, width = q_ref.shape
    row_id = lax.broadcasted_iota(jnp.int32, (rows, rows), 0)
    col_id = lax.broadcasted_iota(jnp.int32, (rows, rows), 1)
    lower = row_id >= col_id
    strict = row_id > col_id
    eye = jnp.where(row_id == col_id, 1.0, 0.0)
    here = range(units)
    query = [unit(silu(q_ref[u].astype(jnp.float32))) * HEAD ** (-0.5) for u in here]
    keys = [unit(silu(k_ref[u].astype(jnp.float32))) for u in here]
    values = [silu(v_ref[u].astype(jnp.float32)) for u in here]
    gamma = [
        jnp.where(lower, jnp.exp(jnp.where(lower, cum_col_ref[u] - cum_row_ref[u], 0.0)), 0.0)
        for u in here
    ]
    k_beta = [keys[u] * beta_ref[u] for u in here]
    a = [jnp.where(strict, mm_nt(k_beta[u], keys[u], HIGH) * gamma[u], 0.0) for u in here]
    size = 1
    t = None
    while size < rows:
        pair = 2 * size
        off = (row_id // pair == col_id // pair) & (row_id % pair >= size) & (col_id % pair < size)
        part = [jnp.where(off, a[u], 0.0) for u in here]
        if t is None:
            t = [eye - part[u] for u in here]
        else:
            half = [mm(part[u], t[u], HIGH) for u in here]
            t = [t[u] - mm(t[u], half[u], HIGH) for u in here]
        size = pair
    for u in here:
        grow = jnp.exp(cum_col_ref[u])
        last = cum_col_ref[u][rows - 1 :, :]
        right = jnp.concatenate([values[u] * beta_ref[u], k_beta[u] * grow], axis=1)
        solved = mm(t[u], right, HIGH)
        q_k = mm_nt(query[u], keys[u]) * gamma[u]
        k_decayed = keys[u] * jnp.exp(last - cum_col_ref[u])
        inner = mm(q_k, solved)
        p_ref[u] = query[u] * grow - inner[:, width:]
        u_ref[u] = inner[:, :width]
        state = mm_tn(k_decayed, solved, HIGH)
        m_ref[u] = eye[:width, :width] * jnp.exp(last) - state[:, width:]
        o_ref[u] = state[:, :width]


def delta_terms(query, keys, values, cum, beta):
    units, rows, width = query.shape
    f32 = jnp.float32
    group = next(g for g in (4, 2, 1) if units % g == 0)

    def spec(*dims):
        return pl.BlockSpec((group,) + dims, lambda i: (i, 0, 0))

    return pl.pallas_call(
        delta_kernel,
        grid=(units // group,),
        out_shape=(
            jax.ShapeDtypeStruct((units, rows, width), f32),
            jax.ShapeDtypeStruct((units, rows, width), f32),
            jax.ShapeDtypeStruct((units, width, width), f32),
            jax.ShapeDtypeStruct((units, width, width), f32),
        ),
        in_specs=[spec(rows, width)] * 3 + [spec(rows, 1), spec(1, rows), spec(rows, 1)],
        out_specs=(spec(rows, width), spec(rows, width), spec(width, width), spec(width, width)),
        compiler_params=pltpu.CompilerParams(vmem_limit_bytes=48 * 1024 * 1024),
        cost_estimate=pl.CostEstimate(
            flops=units * rows * rows * rows * 180, bytes_accessed=units * rows * width * 16, transcendentals=0
        ),
    )(query, keys, values, cum[..., None], cum[:, None, :], beta[..., None])


def on_device(
    cols,
    tokens,
    input_norm_gain,
    query_weight,
    key_weight,
    value_weight,
    decay_gate_weight,
    write_strength_weight,
    up_weight,
    gate_half_weight,
    log_decay_rate,
    write_strength_bias,
    decay_spike_added,
    starting_state,
    head_norm_gain,
    convolution_kernel,
    channel_norm_gain,
    delta_output_rows,
    convolution_output_rows,
):
    rows = tokens.shape[1]
    count = 1
    for axis in cols:
        count *= lax.axis_size(axis)
    channels = convolution_kernel.shape[1]
    taps = convolution_kernel.shape[0]
    tp_index = lax.axis_index("tp")
    sp_index = lax.axis_index("sp")
    col = lax.axis_index(cols) if cols else 0
    heads_tp = query_weight.shape[1] // HEAD
    heads = heads_tp // count
    chan_tp = up_weight.shape[1]
    chan = chan_tp // count
    head_start = tp_index * heads_tp + col * heads
    chan_start = tp_index * chan_tp + col * chan

    def mine(weight, axis, width):
        return lax.dynamic_slice_in_dim(weight, col * width, width, axis)

    wide = heads * HEAD
    stacked = jnp.concatenate(
        [mine(w, 1, wide) for w in (query_weight, key_weight, value_weight)]
        + [mine(w, 1, chan) for w in (up_weight, gate_half_weight)],
        axis=1,
    )
    gathered_in = lax.all_gather(stacked, "sp", axis=0, tiled=True)
    token_all = lax.all_gather(tokens[0], cols + ("tp",), axis=0, tiled=False)
    token_all = token_all.reshape((count, -1, rows, tokens.shape[2]))
    token_all = jnp.swapaxes(token_all, 1, 2).reshape((count * rows, -1))
    out_rows = jnp.concatenate(
        [mine(delta_output_rows, 0, wide), mine(convolution_output_rows, 0, chan)], axis=0
    )
    spikes = decay_spike_added[0]
    start_state = starting_state[0]
    if cols:
        spikes = lax.all_gather(spikes, cols, axis=0, tiled=False)
        start_state = lax.all_to_all(
            start_state.reshape((count, heads, HEAD, HEAD)), cols, 0, 0, tiled=False
        ).reshape((count * heads, HEAD, HEAD))
    spikes = spikes.reshape((count, rows, heads_tp))
    spikes = lax.dynamic_slice_in_dim(spikes, col * heads, heads, 2)

    token_f = token_all.astype(jnp.float32)
    normed = (
        token_f
        * lax.rsqrt(jnp.mean(token_f * token_f, axis=-1, keepdims=True) + EPS)
        * input_norm_gain
    ).astype(jnp.bfloat16)

    gate_cols = jnp.concatenate(
        [
            lax.dynamic_slice_in_dim(decay_gate_weight, head_start, heads, 1),
            lax.dynamic_slice_in_dim(write_strength_weight, head_start, heads, 1),
        ],
        axis=1,
    )
    small = rounded(jnp.dot(normed, gate_cols, preferred_element_type=jnp.float32))
    small = small.reshape((count, rows, 2 * heads))
    rates = jnp.exp(lax.dynamic_slice_in_dim(log_decay_rate, head_start, heads, 0))
    bias = lax.dynamic_slice_in_dim(write_strength_bias, head_start, heads, 0)
    log_decay = -rates * jax.nn.softplus(small[..., :heads]) + spikes
    beta = jax.nn.sigmoid(small[..., heads:] + bias)
    ones = jnp.tril(jnp.ones((rows, rows), jnp.float32))
    cum = jnp.einsum("ij,cjh->chi", ones, log_decay, precision=HIGH).reshape((count * heads, rows))
    beta = jnp.swapaxes(beta, 1, 2).reshape((count * heads, rows))

    raw = jnp.dot(normed, gathered_in, preferred_element_type=jnp.float32).astype(jnp.bfloat16)

    def heads_of(block):
        block = block.reshape((count, rows, heads, HEAD))
        return jnp.swapaxes(block, 1, 2).reshape((count * heads, rows, HEAD))

    p_rows, u_rows, maps, offsets = delta_terms(
        heads_of(raw[:, :wide]),
        heads_of(raw[:, wide : 2 * wide]),
        heads_of(raw[:, 2 * wide : 3 * wide]),
        cum,
        beta,
    )
    up = raw[:, 3 * wide : 3 * wide + chan].astype(jnp.float32)
    gate = raw[:, 3 * wide + chan :].astype(jnp.float32)
    glu = (up * jax.nn.sigmoid(gate)).astype(jnp.bfloat16).reshape((count, rows, chan))
    rim = from_behind(glu[:, rows - (taps - 1) :], "sp", 1)
    first = sp_index == 0
    state = jnp.where(first, start_state, jnp.zeros_like(start_state))
    for _ in range(lax.axis_size("sp") - 1):
        sent = jnp.einsum("hde,hef->hdf", maps, state, precision=HIGH) + offsets
        state = jnp.where(first, start_state, from_behind(sent, "sp", 1))

    extended = jnp.concatenate([rim, glu], axis=1).astype(jnp.float32)
    taps_here = lax.dynamic_slice_in_dim(convolution_kernel, chan_start, chan, 1)
    conv = jnp.zeros((count, rows, chan), jnp.float32)
    for tap in range(taps):
        conv = conv + taps_here[tap] * extended[:, tap : tap + rows]
    sums = jnp.stack([jnp.sum(conv, axis=-1), jnp.sum(conv * conv, axis=-1)])
    sums = lax.psum(sums, cols + ("tp",))
    mean_c = (sums[0] / channels)[..., None]
    var_c = (sums[1] / channels)[..., None] - mean_c * mean_c
    gain = lax.dynamic_slice_in_dim(channel_norm_gain, chan_start, chan, 0)
    conv_out = jax.nn.silu((conv - mean_c) * lax.rsqrt(var_c + EPS) * gain).astype(jnp.bfloat16)

    attn = jnp.einsum("hcd,hde->hce", p_rows, state) + u_rows
    attn_out = (
        attn * lax.rsqrt(jnp.mean(attn * attn, axis=-1, keepdims=True) + EPS) * head_norm_gain
    ).astype(jnp.bfloat16)
    attn_out = jnp.swapaxes(attn_out.reshape((count, heads, rows, HEAD)), 1, 2)
    attn_out = attn_out.reshape((count * rows, wide))
    mixer = jnp.concatenate([attn_out, conv_out.reshape((count * rows, chan))], axis=1)
    gathered_out = lax.all_gather(out_rows, "sp", axis=1, tiled=True)
    term = jnp.dot(mixer, gathered_out, preferred_element_type=jnp.float32).astype(jnp.bfloat16)
    half = term.shape[1] // lax.axis_size("tp")
    term = jnp.swapaxes(term.reshape((count, rows, -1, half)), 1, 2).reshape((-1, rows, half))
    mixed = lax.psum_scatter(term, cols + ("tp",), scatter_dimension=0, tiled=True)
    return mixed


def split_axes(mesh, heads_tp, chan_tp):
    for axes in (("grp", "fs"), ("fs",), ("grp",)):
        count = 1
        for axis in axes:
            count *= mesh.shape[axis]
        if heads_tp % count == 0 and chan_tp % (count * 128) == 0:
            return axes
    return ()


def solution(mesh):
    def whole(*args):
        heads_tp = args[2].shape[1] // HEAD // mesh.shape["tp"]
        chan_tp = args[7].shape[1] // mesh.shape["tp"]
        cols = split_axes(mesh, heads_tp, chan_tp)
        return jax.shard_map(
            functools.partial(on_device, cols),
            mesh=mesh,
            in_specs=(
                P(("grp", "fs"), "sp", "tp"),
                P(),
                P("sp", "tp"),
                P("sp", "tp"),
                P("sp", "tp"),
                P(),
                P(),
                P("sp", "tp"),
                P("sp", "tp"),
                P(),
                P(),
                P(("grp", "fs"), "sp", "tp"),
                P(("grp", "fs"), "tp", None, None),
                P(),
                P(),
                P(),
                P("tp", "sp"),
                P("tp", "sp"),
            ),
            out_specs=P(("grp", "fs"), "sp", "tp"),
            check_vma=False,
        )(*args)

    return whole
```

time: 377 us -> 268 us (0.71)
  other arithmetic: 89.8 us -> 7.79 us
  waiting for transfers between devices: 183 us -> 107 us
  local copies, waits for them, and re-layouts: 8.34 us -> 47.8 us
  matrix products: 50.6 us -> 29.8 us
  blocking collectives: 2.47 us -> 22 us
  Pallas kernels: 0 us -> 17.1 us
  starting transfers between devices: 26.9 us -> 18 us
    all_gather x8 -> x3, waiting for transfers between devices: 142 us -> 49.2 us  [the longest x1 34.6 us: on_device(): gathered_in = lax.all_gather(stacked, 'sp', axis=0, tiled=True)]
    another operation x3 -> x1, other arithmetic: 79.6 us -> 0.01 us  [on_device(): sums = jnp.stack([jnp.sum(conv, axis=-1), jnp.sum(conv * conv, axis=-1)])]
    reduce_scatter x1, waiting for transfers between devices: 7.96 us -> 50.8 us  [on_device(): lax.psum_scatter(term, cols + ('tp',), scatter_dimension=0, tiled=True)]
    ppermute x4, waiting for transfers between devices: 28.4 us -> 6.05 us  [from_behind(): return lax.ppermute(block, axis, route)]
    dot_general x44 -> x7, matrix products: 47.8 us -> 28.4 us  [the longest x1 18.4 us: on_device(): jnp.dot(normed, gathered_in, preferred_element_type=jnp.float32)]
    pallas_call x0 -> x1, Pallas kernels: none -> 17.1 us  [delta_terms(): pl.pallas_call(delta_kernel, grid=(units // group,), out_shape=(jax.Shape...]
    unnamed x98 -> x27, local copies, waits for them, and re-layouts: 0.22 us -> 16 us
    ppermute x4, starting transfers between devices: 26.6 us -> 12.7 us  [from_behind(): return lax.ppermute(block, axis, route)]
  transfers between devices with their start and end apart: 13 -> 9, of which waited for: 9 -> 5; matrix products, arithmetic and copies ran while one was open for 39% -> 25% of each run, Pallas kernels for 0% -> 6%
where the time goes in v1:
time: 268 us; the launch traced here: 264 us
  waiting for transfers between devices  107 us (40%)
  local copies, waits for them, and re-layouts  47.8 us (18%)
  matrix products  29.8 us (11%)
  blocking collectives  22 us (8%)
  starting transfers between devices  18 us (7%)
  Pallas kernels  17.1 us (6%)
  between operations  14.5 us (5%)
  other arithmetic  7.79 us (3%)
    reduce_scatter x1, waiting for transfers between devices, on_device(): lax.psum_scatter(term, cols + ('tp',), scatter_dimension=0, tiled=True)  50.8 us
    all_gather x1, waiting for transfers between devices, on_device(): gathered_in = lax.all_gather(stacked, 'sp', axis=0, tiled=True)  34.6 us
    dot_general x1, matrix products, on_device(): jnp.dot(normed, gathered_in, preferred_element_type=jnp.float32)  18.4 us
    pallas_call x1, Pallas kernels, delta_terms(): pl.pallas_call(delta_kernel, grid=(units // group,), out_shape=(jax.Shape...  17.1 us
    unnamed x27, local copies, waits for them, and re-layouts  16 us
    all_gather x1, waiting for transfers between devices, on_device(): token_all = lax.all_gather(tokens[0], cols + ('tp',), axis=0, tiled=False)  14.6 us
    psum x1, blocking collectives, on_device(): sums = lax.psum(sums, cols + ('tp',))  13.1 us
    ppermute x4, starting transfers between devices, from_behind(): return lax.ppermute(block, axis, route)  12.7 us
  transfers between devices with their start and end apart: 9, of which 5 were waited for; matrix products, arithmetic and copies ran while one was open for 25% of the time, Pallas kernels for 6%

profile of v1, /device:TPU:0, one launch (start us, length us, event | category | flops | bytes accessed | tf_op | source)
XLA Modules:
  0.0 263.6 jit_solution(13944216638870865558)
XLA Ops:
  6.5 0.7 all-gather.4.cloned.1.call-update
  7.3 0.9 dynamic-slice_dynamic-update-slice_fusion.4
  8.3 0.9 dynamic-slice_dynamic-update-slice_fusion.3
  9.2 0.9 dynamic-slice_dynamic-update-slice_fusion.2
  10.1 0.9 dynamic-slice_dynamic-update-slice_fusion.1
  11.1 0.9 dynamic-slice_dynamic-update-slice_fusion
  12.0 0.9 copy-done.3
  13.0 5.2 %all-to-all-start = ((f32[4,1,128,128]{3,2,1,0:T(8,128)}), f32[4,1,128,128]{3,2,1,0:T(8,128)}, u32[]{:S(2)}, u32[]{:S(2)}) async-start(f32[4,1,128,128]{3,2,1,0:T(8,128)} %bitcast.130), calls=%async_computation | async-start | bytes 524288 | tf_op jit(solution)/shard_map/all_to_all | solution.py:176
  18.2 1.0 constant_dynamic-slice_fusion.1
  19.2 0.7 pad_maximum_fusion
  20.0 0.6 dynamic_slice.47
  21.2 0.7 dynamic_slice.51
  21.9 8.9 %all_gather.14 = f32[4,256,4]{1,2,0:T(4,128)S(1)} all-gather(f32[1,256,4]{1,2,0:T(4,128)S(1)} %copy-done.5), channel_id=1, replica_groups=mesh['grp'=2,'sp'=4,'fs'=2,'tp'=2] {'grp','fs'}, dimensions={0}, use_global_device_ids=true | all-gather | bytes 20480 | tf_op jit(solution)/shard_map/all_gather | solution.py:175
  30.8 0.2 copy.52
  31.0 0.8 constant_dynamic-slice_fusion.4
  31.8 1.3 dynamic_slice.53
  33.1 1.6 dynamic-slice_bitcast_fusion.29
  34.8 1.2 fusion.57
  36.0 14.6 %all-gather.4.cloned.1.call-done = bf16[8,256,1024]{2,1,0:T(8,128)(2,1)} async-done(((bf16[1,256,1024]{2,1,0:T(8,128)(2,1)}), bf16[8,256,1024]{2,1,0:T(8,128)(2,1)}) %all-gather.4.cloned.1.call-update) | async-done | bytes 4194320 | tf_op jit(solution)/shard_map/all_gather | solution.py:166
  50.5 9.8 %copy.43 = f32[4,2,256,1024]{3,1,2,0:T(2,128)} copy(bf16[4,2,256,1024]{3,2,1,0:T(8,128)(2,1)} %bitcast.122) | data formatting | bytes 12582912 | tf_op jit(solution)/shard_map/convert_element_type | solution.py:182
  60.3 11.0 %copy.53 = f32[128,8,2,1024]{3,1,2,0:T(8,128)} copy(f32[128,8,2,1024]{3,2,1,0:T(2,128)} %bitcast.121) | data formatting | bytes 16777216
  71.3 0.9 multiply_reduce_fusion
  72.3 34.6 %all-gather.6.cloned.1.call-done = bf16[2048,640]{1,0:T(8,128)(2,1)} async-done(((bf16[512,640]{1,0:T(8,128)(2,1)}), bf16[2048,640]{1,0:T(8,128)(2,1)}) %all-gather.6.cloned.1.call-update) | async-done | bytes 2621456 | tf_op jit(solution)/shard_map/all_gather | solution.py:165
  106.9 18.4 %convolution_convert_fusion.1 = bf16[1024,640]{1,0:T(8,128)(2,1)S(1)} fusion(bf16[2048,640]{1,0:T(8,128)(2,1)} %all-gather.6.cloned.1.call-done, f32[1024,2048]{1,0:T(8,128)} %bitcast.119, f32[2048]{0:T(1024)S(1)} %copy-done.4, f32[1024]{0:T(1024)S(1)} %bitcast.131), kind=kOutput, calls=%fused_computation.3 | convolution fusion | flops 2691301376 | bytes 12333056 | tf_op jit(solution)/shard_map/dot_general | solution.py:206
  125.6 1.3 convolution_convert_fusion.2
  127.1 1.3 fusion.36
  128.4 0.3 fusion.40
  128.7 0.2 copy.49.cum_col_ref
  129.0 1.7 collective-permute-start.3
  130.7 17.1 %shard_map.172 = (f32[4,256,128]{2,1,0:T(8,128)S(1)}, f32[4,256,128]{2,1,0:T(8,128)S(1)}, f32[4,128,128]{2,1,0:T(8,128)S(1)}, f32[4,128,128]{2,1,0:T(8,128)S(1)}) custom-call(bf16[4,256,128]{2,1,0:T(8,128)(2,1)S(1)} %bitcast.118, bf16[4,256,128]{2,1,0:T(8,128)(2,1)S(1)} %bitcast.117, bf16[4,256,128]{2,1,0:T(8,128)(2,1)S(1)} %bitcast.116, ...), custom_call_target="tpu_custom_call" | custom-call | flops 12079595520 | bytes 2097152 | tf_op jit(solution)/shard_map/pallas_call | solution.py:101
  147.8 1.3 convolution_add_fusion.3
  149.1 3.9 %collective-permute-start = (f32[4,128,128]{2,1,0:T(8,128)S(1)}, f32[4,128,128]{2,1,0:T(8,128)S(1)}, u32[]{:S(2)}, u32[]{:S(2)}) collective-permute-start(f32[4,128,128]{2,1,0:T(8,128)S(1)} %convolution_add_fusion.3), channel_id=1, source_target_pairs={{0,4},{4,8},{8,12},{1,5},{5,9},{9,13},{2,6},{6,10},{10,14},{3,7},{... | collective-permute-start | bytes 786440 | tf_op jit(solution)/shard_map/ppermute | solution.py:18
  153.0 1.0 maximum_convert_fusion
  154.0 3.1 %fusion.63 = (f32[4,256]{1,0:T(4,128)S(1)}, f32[4,256]{1,0:T(4,128)S(1)}, f32[4,256,128]{2,1,0:T(8,128)S(1)}) fusion(f32[4,286,128]{2,1,0:T(8,128)S(1)} %maximum_convert_fusion, f32[128]{0:T(128)} %get-tuple-element.51, f32[128]{0:T(128)S(1)} %get-tuple-element.22, f32[128]{0:T(128)S(1)} %get-tuple-element.23, f32[128]{0:T(128)S(1)} %get-tuple-element.24, ...), kind=kLoop, calls=%fused_computation.163 | loop fusion | flops 8386560 | bytes 16801280 | tf_op jit(solution)/shard_map/reduce_sum | solution.py:234
  157.2 13.1 %psum.7 = f32[2,4,256]{2,1,0:T(4,128)S(1)} all-reduce(f32[2,4,256]{2,1,0:T(4,128)S(1)} %pad_maximum_fusion.1), channel_id=1, replica_groups=mesh['grp'=2,'sp'=4,'fs'=2,'tp'=2] {'grp','fs','tp'}, use_global_device_ids=true, to_apply=%region_5.6 | all-reduce | flops 2048 | bytes 16384 | tf_op jit(solution)/shard_map/psum | solution.py:235
  170.3 1.3 convolution_add_fusion.2
  171.7 2.7 %collective-permute-start.1 = (f32[4,128,128]{2,1,0:T(8,128)S(1)}, f32[4,128,128]{2,1,0:T(8,128)S(1)}, u32[]{:S(2)}, u32[]{:S(2)}) collective-permute-start(f32[4,128,128]{2,1,0:T(8,128)S(1)} %convolution_add_fusion.2), channel_id=1, source_target_pairs={{0,4},{4,8},{8,12},{1,5},{5,9},{9,13},{2,6},{6,10},{10,14},{3,7},{... | collective-permute-start | bytes 786440 | tf_op jit(solution)/shard_map/ppermute | solution.py:18
  174.4 3.9 %collective-permute-done.1 = f32[4,128,128]{2,1,0:T(8,128)S(1)} collective-permute-done((f32[4,128,128]{2,1,0:T(8,128)S(1)}, f32[4,128,128]{2,1,0:T(8,128)S(1)}, u32[]{:S(2)}, u32[]{:S(2)}) %collective-permute-start.1) | collective-permute-done | bytes 262176 | tf_op jit(solution)/shard_map/ppermute | solution.py:18
  178.3 1.4 convolution_add_fusion.1
  179.7 4.4 %collective-permute-start.2 = (bf16[4,128,128]{2,1,0:T(8,128)(2,1)S(1)}, bf16[4,128,128]{2,1,0:T(8,128)(2,1)S(1)}, u32[]{:S(2)}, u32[]{:S(2)}) collective-permute-start(bf16[4,128,128]{2,1,0:T(8,128)(2,1)S(1)} %convolution_add_fusion.1), channel_id=1, source_target_pairs={{0,4},{4,8},{8,12},{1,5},{5,9},{9,13},{2,6},{6,10},{10,14},{3,7},{... | collective-permute-start | bytes 393224 | tf_op jit(solution)/shard_map/ppermute | solution.py:18
  184.1 0.4 multiply_convert_fusion.1
  184.5 2.1 collective-permute-done.2
  186.6 1.3 multiply_reduce_fusion.2
  187.9 0.2 multiply_convert_fusion.3
  188.2 4.4 %convolution_convert_fusion = bf16[1024,2048]{1,0:T(8,128)(2,1)} fusion(bf16[256,2048]{1,0:T(8,128)(2,1)} %all-gather.8.cloned.1.call-done, bf16[1024,128]{1,0:T(8,128)(2,1)S(1)} %bitcast.128, bf16[1024,128]{1,0:T(8,128)(2,1)S(1)} %bitcast.129), kind=kOutput, calls=%fused_computation.2 | convolution fusion | flops 1076887552 | bytes 5767168 | tf_op jit(solution)/shard_map/dot_general | solution.py:249
  192.6 7.8 %reshape.131 = bf16[4,256,2,1024]{3,2,1,0:T(2,128)(2,1)} reshape(bf16[1024,2048]{1,0:T(8,128)(2,1)} %convolution_convert_fusion) | data formatting | bytes 8388608 | tf_op jit(solution)/shard_map/reshape | solution.py:251
  200.4 5.5 %copy.50 = bf16[4,2,256,1024]{3,2,1,0:T(8,128)(2,1)} copy(bf16[4,2,256,1024]{3,1,2,0:T(2,128)(2,1)} %bitcast.124) | data formatting | bytes 8388608 | tf_op jit(solution)/shard_map/transpose | solution.py:251
  205.9 50.8 %reduce-scatter.2.cloned.1.call-done = bf16[1,256,1024]{2,1,0:T(8,128)(2,1)} async-done(((bf16[8,256,1024]{2,1,0:T(8,128)(2,1)}), bf16[1,256,1024]{2,1,0:T(8,128)(2,1)}) %reduce-scatter.2.cloned.1.call-update) | async-done | bytes 524304 | tf_op jit(solution)/shard_map/reduce_scatter | solution.py:252
  (44 shorter events, 0.8 us)
Async XLA Ops:
  6.5 13.5 %copy-start.8 = (f32[8]{0:T(128)S(1)}, f32[8]{0:T(128)}, u32[]{:S(2)}) copy-start(f32[8]{0:T(128)} %param.27) | copy-start | bytes 100
  6.5 14.7 %copy-start.9 = (f32[8]{0:T(128)S(1)}, f32[8]{0:T(128)}, u32[]{:S(2)}) copy-start(f32[8]{0:T(128)} %param.28) | copy-start | bytes 100
  6.5 15.3 %copy-start.5 = (f32[1,256,4]{1,2,0:T(4,128)S(1)}, f32[1,256,4]{1,2,0:T(4,128)}, u32[]{:S(2)}) copy-start(f32[1,256,4]{1,2,0:T(4,128)} %param.29) | copy-start | bytes 12292
  6.5 44.0 %all-gather.4.cloned.1.call-start = ((), (), s32[]{:S(2)}) async-start(), calls=%async_computation.2 | async-start | bytes 4718592 | tf_op jit(solution)/shard_map/all_gather | solution.py:166
  7.3 99.6 %all-gather.6.cloned.1.call-start = ((), (), s32[]{:S(2)}) async-start(), calls=%async_computation.3 | async-start | bytes 3276800 | tf_op jit(solution)/shard_map/all_gather | solution.py:165
  12.0 0.9 copy-start.3
  13.0 134.8 %all-to-all-start = ((f32[4,1,128,128]{3,2,1,0:T(8,128)}), f32[4,1,128,128]{3,2,1,0:T(8,128)}, u32[]{:S(2)}, u32[]{:S(2)}) async-start(f32[4,1,128,128]{3,2,1,0:T(8,128)} %bitcast.130), calls=%async_computation | async-start | bytes 524288 | tf_op jit(solution)/shard_map/all_to_all | solution.py:176
  18.2 170.0 %all-gather.8.cloned.1.call-start = ((), (), s32[]{:S(2)}) async-start(), calls=%async_computation.4 | async-start | bytes 1310720 | tf_op jit(solution)/shard_map/all_gather | solution.py:248
  19.9 236.8 %reduce-scatter.2.cloned.1.call-start = ((), (), s32[]{:S(2)}) async-start(), calls=%async_computation.5 | async-start | bytes 4718592 | tf_op jit(solution)/shard_map/reduce_scatter | solution.py:252
  60.3 11.0 %copy-start.1 = (bf16[8,256,1024]{2,1,0:T(8,128)(2,1)S(1)}, bf16[8,256,1024]{2,1,0:T(8,128)(2,1)}, u32[]{:S(2)}) copy-start(bf16[8,256,1024]{2,1,0:T(8,128)(2,1)} %all-gather.4.cloned.1.call-done) | copy-start | bytes 12582916
  71.3 35.5 %copy-start.4 = (f32[2048]{0:T(1024)S(1)}, f32[2048]{0:T(1024)}, u32[]{:S(2)}) copy-start(f32[2048]{0:T(1024)} %param.19) | copy-start | bytes 24580
  106.9 18.7 %copy-start = (f32[128,8,2,1024]{3,1,2,0:T(8,128)S(1)}, f32[128,8,2,1024]{3,1,2,0:T(8,128)}, u32[]{:S(2)}) copy-start(f32[128,8,2,1024]{3,1,2,0:T(8,128)} %copy.53) | copy-start | bytes 25165828
  125.6 3.4 %copy-start.2 = (bf16[1024,128]{1,0:T(8,128)(2,1)}, bf16[1024,128]{1,0:T(8,128)(2,1)S(1)}, u32[]{:S(2)}) copy-start(bf16[1024,128]{1,0:T(8,128)(2,1)S(1)} %multiply_convert_fusion.2) | copy-start | bytes 786436
  129.0 24.0 %collective-permute-start.3 = (bf16[4,30,128]{2,1,0:T(8,128)(2,1)S(1)}, bf16[4,30,128]{2,1,0:T(8,128)(2,1)S(1)}, u32[]{:S(2)}, u32[]{:S(2)}) collective-permute-start(bf16[4,30,128]{2,1,0:T(8,128)(2,1)S(1)} %slice.295), channel_id=1, source_target_pairs={{0,4},{4,8},{8,12},{1,5},{5,9},{9,13},{2,6},{6,10},{10,14},{3,7},{... | collective-permute-start | bytes 92168 | tf_op jit(solution)/shard_map/ppermute | solution.py:18
  149.1 21.2 %collective-permute-start = (f32[4,128,128]{2,1,0:T(8,128)S(1)}, f32[4,128,128]{2,1,0:T(8,128)S(1)}, u32[]{:S(2)}, u32[]{:S(2)}) collective-permute-start(f32[4,128,128]{2,1,0:T(8,128)S(1)} %convolution_add_fusion.3), channel_id=1, source_target_pairs={{0,4},{4,8},{8,12},{1,5},{5,9},{9,13},{2,6},{6,10},{10,14},{3,7},{... | collective-permute-start | bytes 786440 | tf_op jit(solution)/shard_map/ppermute | solution.py:18
  154.0 30.1 %copy-start.7 = (f32[128]{0:T(128)S(1)}, f32[128]{0:T(128)}, u32[]{:S(2)}) copy-start(f32[128]{0:T(128)} %dynamic_slice.53) | copy-start | bytes 1540
  157.2 30.8 %copy-start.6 = (f32[128]{0:T(128)S(1)}, f32[128]{0:T(128)}, u32[]{:S(2)}) copy-start(f32[128]{0:T(128)} %param.31) | copy-start | bytes 1540
  171.7 6.6 %collective-permute-start.1 = (f32[4,128,128]{2,1,0:T(8,128)S(1)}, f32[4,128,128]{2,1,0:T(8,128)S(1)}, u32[]{:S(2)}, u32[]{:S(2)}) collective-permute-start(f32[4,128,128]{2,1,0:T(8,128)S(1)} %convolution_add_fusion.2), channel_id=1, source_target_pairs={{0,4},{4,8},{8,12},{1,5},{5,9},{9,13},{2,6},{6,10},{10,14},{3,7},{... | collective-permute-start | bytes 786440 | tf_op jit(solution)/shard_map/ppermute | solution.py:18
  179.7 6.9 %collective-permute-start.2 = (bf16[4,128,128]{2,1,0:T(8,128)(2,1)S(1)}, bf16[4,128,128]{2,1,0:T(8,128)(2,1)S(1)}, u32[]{:S(2)}, u32[]{:S(2)}) collective-permute-start(bf16[4,128,128]{2,1,0:T(8,128)(2,1)S(1)} %convolution_add_fusion.1), channel_id=1, source_target_pairs={{0,4},{4,8},{8,12},{1,5},{5,9},{9,13},{2,6},{6,10},{10,14},{3,7},{... | collective-permute-start | bytes 393224 | tf_op jit(solution)/shard_map/ppermute | solution.py:18
Sparse Core Ops, SparseCore 0:
  9.2 41.2 all-gather.3
  52.1 54.7 all-gather.5
  108.4 26.7 all-gather.7
  206.0 50.6 reduce-scatter.1

commit v2 on v1

--- a/solution.py
+++ b/solution.py
@@ -44,6 +44,275 @@
 
 def unit(x):
     return x * lax.rsqrt(jnp.sum(x * x, axis=-1, keepdims=True) + EPS)
+
+
+MESH = pl.DeviceIdType.MESH
+
+
+def column_peer(cols, sizes, index):
+    where = {}
+    for axis, size in reversed(list(zip(cols, sizes))):
+        where[axis] = lax.rem(index, size)
+        index = index // size
+    return where
+
+
+def column_index(cols, sizes):
+    index = 0
+    for axis, size in zip(cols, sizes):
+        index = index * size + lax.axis_index(axis)
+    return index
+
+
+def greet(peers):
+    barrier = pltpu.get_barrier_semaphore()
+    for peer in peers:
+        pl.semaphore_signal(barrier, inc=1, device_id=peer, device_id_type=MESH)
+    pl.semaphore_wait(barrier, len(peers))
+
+
+def send(src, dst, send_sem, recv_sem, peer):
+    copy = pltpu.make_async_remote_copy(
+        src_ref=src, dst_ref=dst, send_sem=send_sem, recv_sem=recv_sem, device_id=peer, device_id_type=MESH
+    )
+    copy.start()
+    return copy
+
+
+def gather_kernel(
+    cols, sizes, ring, tok_ref, w_ref, spike_ref, state_ref, gain_ref, gates_ref,
+    raw_ref, small_ref, spikes_ref, states_ref,
+    tok_all, w_all, normed,
+    tok_send, tok_recv, fwd_send, fwd_recv, w_send, w_recv, spk_send, spk_recv, st_send, st_recv, local_sem,
+):
+    rows, half = tok_ref.shape
+    depth = w_ref.shape[0]
+    count = 1
+    for size in sizes:
+        count *= size
+    col = column_index(cols, sizes)
+    tp = lax.axis_index("tp")
+    sp = lax.axis_index("sp")
+    partner = {"tp": 1 - tp}
+    peers = [column_peer(cols, sizes, lax.rem(col + d, count)) for d in range(count)]
+    right = {"sp": lax.rem(sp + 1, ring)}
+    left = {"sp": lax.rem(sp + ring - 1, ring)}
+
+    def place(source, side):
+        return tok_all.at[
+            pl.ds(pl.multiple_of(source * rows, rows), rows), pl.ds(pl.multiple_of(side * half, half), half)
+        ]
+
+    mid = depth // 2
+
+    def shard(owner, top):
+        begin = owner * depth + (0 if top else mid)
+        return w_all.at[pl.ds(pl.multiple_of(begin, mid), mid), :]
+
+    own = pltpu.make_async_copy(tok_ref, place(col, tp), local_sem.at[0])
+    own.start()
+    own_w = pltpu.make_async_copy(
+        w_ref, w_all.at[pl.ds(pl.multiple_of(sp * depth, depth), depth), :], local_sem.at[1]
+    )
+    own_w.start()
+    own_spike = pltpu.make_async_copy(spike_ref, spikes_ref.at[col], local_sem.at[2])
+    own_spike.start()
+    own_state = pltpu.make_async_copy(state_ref.at[col], states_ref.at[col], local_sem.at[3])
+    own_state.start()
+    greet([right, left, partner] + peers[1:])
+
+    fwd = {0: send(tok_ref, place(col, tp), fwd_send.at[0], fwd_recv.at[0], partner)}
+    w_copies = []
+
+    def ring_step(step):
+        behind = lax.rem(sp - step + ring, ring)
+        ahead = lax.rem(sp + step, ring)
+        top = w_ref.at[pl.ds(0, mid), :] if step == 0 else shard(behind, True)
+        low = w_ref.at[pl.ds(mid, mid), :] if step == 0 else shard(ahead, False)
+        w_copies.append(
+            (
+                send(top, shard(behind, True), w_send.at[0, step], w_recv.at[0, step], right),
+                send(low, shard(ahead, False), w_send.at[1, step], w_recv.at[1, step], left),
+            )
+        )
+
+    if ring > 1:
+        ring_step(0)
+    toks, spikes, states = {}, {}, {}
+    for d in range(1, count):
+        peer = peers[d]
+        spikes[d] = send(spike_ref, spikes_ref.at[col], spk_send.at[d], spk_recv.at[d], peer)
+        toks[d] = send(tok_ref, place(col, tp), tok_send.at[d], tok_recv.at[d], peer)
+    for d in range(1, count):
+        target = lax.rem(col + d, count)
+        states[d] = send(state_ref.at[target], states_ref.at[col], st_send.at[d], st_recv.at[d], peers[d])
+
+    def normalise(source):
+        span = pl.ds(pl.multiple_of(source * rows, rows), rows)
+        block = tok_all[span, :].astype(jnp.float32)
+        scale = lax.rsqrt(jnp.mean(block * block, axis=-1, keepdims=True) + EPS)
+        normed[span, :] = (block * scale * gain_ref[...]).astype(jnp.bfloat16)
+
+    own.wait()
+    fwd[0].wait()
+    normalise(col)
+    for i in range(max(ring - 1, count - 1)):
+        if i < ring - 1:
+            for copy in w_copies[i]:
+                copy.wait()
+            if i + 1 < ring - 1:
+                ring_step(i + 1)
+        d = i + 1
+        if d < count:
+            toks[d].wait()
+            source = lax.rem(col - d + count, count)
+            fwd[d] = send(place(source, tp), place(source, tp), fwd_send.at[d], fwd_recv.at[d], partner)
+            if d > 1:
+                fwd[d - 1].wait()
+                normalise(lax.rem(col - d + 1 + count, count))
+    if count > 1:
+        fwd[count - 1].wait()
+        normalise(lax.rem(col + 1, count))
+    own_w.wait()
+    own_spike.wait()
+    own_state.wait()
+    for d in range(1, count):
+        spikes[d].wait()
+        states[d].wait()
+
+    @pl.loop(0, count)
+    def _(c):
+        span = pl.ds(pl.multiple_of(c * rows, rows), rows)
+        block = normed[span, :]
+        raw_ref[span, :] = mm(block, w_all[...]).astype(jnp.bfloat16)
+        small_ref[span, :] = mm(block, gates_ref[...])
+
+
+def gather_project(cols, sizes, ring, tokens, weights, spikes, states, gain, gates):
+    rows, half = tokens.shape
+    depth, width = weights.shape
+    count = states.shape[0]
+    total = depth * ring
+    dma = pltpu.SemaphoreType.DMA
+    vmem = pl.BlockSpec(memory_space=pltpu.VMEM)
+    anywhere = pl.BlockSpec(memory_space=pl.ANY)
+    return pl.pallas_call(
+        functools.partial(gather_kernel, cols, sizes, ring),
+        out_shape=(
+            jax.ShapeDtypeStruct((count * rows, width), jnp.bfloat16),
+            jax.ShapeDtypeStruct((count * rows, gates.shape[1]), jnp.float32),
+            jax.ShapeDtypeStruct((count,) + spikes.shape, jnp.float32),
+            jax.ShapeDtypeStruct(states.shape, jnp.float32),
+        ),
+        in_specs=[anywhere, anywhere, vmem, vmem, vmem, vmem],
+        out_specs=(vmem,) * 4,
+        scratch_shapes=[
+            pltpu.VMEM((count * rows, total), jnp.bfloat16),
+            pltpu.VMEM((total, width), jnp.bfloat16),
+            pltpu.VMEM((count * rows, total), jnp.bfloat16),
+            dma((count,)), dma((count,)), dma((count,)), dma((count,)),
+            dma((2, ring)), dma((2, ring)),
+            dma((count,)), dma((count,)), dma((count,)), dma((count,)),
+            dma((4,)),
+        ],
+        compiler_params=pltpu.CompilerParams(
+            collective_id=1, has_side_effects=True, vmem_limit_bytes=48 * 1024 * 1024
+        ),
+        name="gather_project",
+    )(tokens, weights, spikes, states, gain, gates)
+
+
+def sum_kernel(cols, sizes, x_ref, o_ref, slots, send_sem, recv_sem):
+    count = slots.shape[0]
+    names, widths = cols + ("tp",), sizes + (2,)
+    me = column_index(names, widths)
+    peers = [column_peer(names, widths, lax.rem(me + d, count)) for d in range(count)]
+    greet(peers[1:])
+    copies = [
+        send(x_ref, slots.at[d], send_sem.at[d], recv_sem.at[d], peers[d]) for d in range(1, count)
+    ]
+    total = x_ref[...]
+    for d in range(1, count):
+        copies[d - 1].wait()
+        total = total + slots[d]
+    o_ref[...] = total
+
+
+def sum_small(cols, sizes, x):
+    count = 2
+    for size in sizes:
+        count *= size
+    return pl.pallas_call(
+        functools.partial(sum_kernel, cols, sizes),
+        out_shape=jax.ShapeDtypeStruct(x.shape, x.dtype),
+        in_specs=[pl.BlockSpec(memory_space=pltpu.VMEM)],
+        out_specs=pl.BlockSpec(memory_space=pltpu.VMEM),
+        scratch_shapes=[
+            pltpu.VMEM((count,) + x.shape, x.dtype),
+            pltpu.SemaphoreType.DMA((count,)),
+            pltpu.SemaphoreType.DMA((count,)),
+        ],
+        compiler_params=pltpu.CompilerParams(collective_id=2, has_side_effects=True),
+        name="sum_small",
+    )(x)
+
+
+def project_kernel(
+    cols, sizes, mix_ref, w_ref, out_ref, to_pair, from_pair, to_col, from_col,
+    pair_send, pair_recv, col_send, col_recv,
+):
+    count, rows, half = from_col.shape
+    col = column_index(cols, sizes)
+    tp = lax.axis_index("tp")
+    partner = {"tp": 1 - tp}
+    peers = [column_peer(cols, sizes, lax.rem(col + d, count)) for d in range(count)]
+    greet([partner] + peers[1:])
+    order = [d for d in range(1, count)] + [0]
+
+    def part(d, side):
+        target = lax.rem(col + d, count)
+        block = mix_ref[pl.ds(pl.multiple_of(target * rows, rows), rows), :]
+        return mm(block, w_ref[:, pl.ds(pl.multiple_of(side * half, half), half)])
+
+    pairs, sends = {}, {}
+
+    def to_partner(d):
+        to_pair[d] = part(d, 1 - tp).astype(jnp.bfloat16)
+        pairs[d] = send(to_pair.at[d], from_pair.at[d], pair_send.at[d], pair_recv.at[d], partner)
+
+    to_partner(order[0])
+    for i, d in enumerate(order):
+        if i + 1 < count:
+            to_partner(order[i + 1])
+        mine = part(d, tp)
+        pairs[d].wait()
+        mine = mine + from_pair[d].astype(jnp.float32)
+        if d:
+            to_col[d] = mine.astype(jnp.bfloat16)
+            sends[d] = send(to_col.at[d], from_col.at[d], col_send.at[d], col_recv.at[d], peers[d])
+    total = mine
+    for d in range(1, count):
+        sends[d].wait()
+        total = total + from_col[d].astype(jnp.float32)
+    out_ref[...] = total.astype(jnp.bfloat16)
+
+
+def project_out(cols, sizes, rows, mixer, weights):
+    count = mixer.shape[0] // rows
+    half = weights.shape[1] // 2
+    bf16 = jnp.bfloat16
+    dma = pltpu.SemaphoreType.DMA
+    return pl.pallas_call(
+        functools.partial(project_kernel, cols, sizes),
+        out_shape=jax.ShapeDtypeStruct((rows, half), bf16),
+        in_specs=[pl.BlockSpec(memory_space=pltpu.VMEM)] * 2,
+        out_specs=pl.BlockSpec(memory_space=pltpu.VMEM),
+        scratch_shapes=[pltpu.VMEM((count, rows, half), bf16)] * 4 + [dma((count,))] * 4,
+        compiler_params=pltpu.CompilerParams(
+            collective_id=3, has_side_effects=True, vmem_limit_bytes=48 * 1024 * 1024
+        ),
+        name="project_out",
+    )(mixer, weights)
 
 
 def delta_kernel(q_ref, k_ref, v_ref, cum_col_ref, cum_row_ref, beta_ref, p_ref, u_ref, m_ref, o_ref):
@@ -162,30 +431,10 @@
         + [mine(w, 1, chan) for w in (up_weight, gate_half_weight)],
         axis=1,
     )
-    gathered_in = lax.all_gather(stacked, "sp", axis=0, tiled=True)
-    token_all = lax.all_gather(tokens[0], cols + ("tp",), axis=0, tiled=False)
-    token_all = token_all.reshape((count, -1, rows, tokens.shape[2]))
-    token_all = jnp.swapaxes(token_all, 1, 2).reshape((count * rows, -1))
     out_rows = jnp.concatenate(
         [mine(delta_output_rows, 0, wide), mine(convolution_output_rows, 0, chan)], axis=0
     )
-    spikes = decay_spike_added[0]
-    start_state = starting_state[0]
-    if cols:
-        spikes = lax.all_gather(spikes, cols, axis=0, tiled=False)
-        start_state = lax.all_to_all(
-            start_state.reshape((count, heads, HEAD, HEAD)), cols, 0, 0, tiled=False
-        ).reshape((count * heads, HEAD, HEAD))
-    spikes = spikes.reshape((count, rows, heads_tp))
-    spikes = lax.dynamic_slice_in_dim(spikes, col * heads, heads, 2)
-
-    token_f = token_all.astype(jnp.float32)
-    normed = (
-        token_f
-        * lax.rsqrt(jnp.mean(token_f * token_f, axis=-1, keepdims=True) + EPS)
-        * input_norm_gain
-    ).astype(jnp.bfloat16)
-
+    sizes = tuple(lax.axis_size(axis) for axis in cols)
     gate_cols = jnp.concatenate(
         [
             lax.dynamic_slice_in_dim(decay_gate_weight, head_start, heads, 1),
@@ -193,8 +442,22 @@
         ],
         axis=1,
     )
-    small = rounded(jnp.dot(normed, gate_cols, preferred_element_type=jnp.float32))
-    small = small.reshape((count, rows, 2 * heads))
+    gate_cols = jnp.pad(gate_cols, ((0, 0), (0, 128 - 2 * heads)))
+    raw, small, spikes, start_state = gather_project(
+        cols,
+        sizes,
+        lax.axis_size("sp"),
+        tokens[0],
+        stacked,
+        decay_spike_added[0].T.reshape((-1, 128)),
+        starting_state[0].reshape((count, heads * HEAD, HEAD)),
+        input_norm_gain[None],
+        gate_cols,
+    )
+    start_state = start_state.reshape((count * heads, HEAD, HEAD))
+    spikes = spikes.reshape((count, heads_tp, rows))
+    spikes = jnp.swapaxes(lax.dynamic_slice_in_dim(spikes, col * heads, heads, 1), 1, 2)
+    small = rounded(small[:, : 2 * heads]).reshape((count, rows, 2 * heads))
     rates = jnp.exp(lax.dynamic_slice_in_dim(log_decay_rate, head_start, heads, 0))
     bias = lax.dynamic_slice_in_dim(write_strength_bias, head_start, heads, 0)
     log_decay = -rates * jax.nn.softplus(small[..., :heads]) + spikes
@@ -202,8 +465,6 @@
     ones = jnp.tril(jnp.ones((rows, rows), jnp.float32))
     cum = jnp.einsum("ij,cjh->chi", ones, log_decay, precision=HIGH).reshape((count * heads, rows))
     beta = jnp.swapaxes(beta, 1, 2).reshape((count * heads, rows))
-
-    raw = jnp.dot(normed, gathered_in, preferred_element_type=jnp.float32).astype(jnp.bfloat16)
 
     def heads_of(block):
         block = block.reshape((count, rows, heads, HEAD))
@@ -232,7 +493,7 @@
     for tap in range(taps):
         conv = conv + taps_here[tap] * extended[:, tap : tap + rows]
     sums = jnp.stack([jnp.sum(conv, axis=-1), jnp.sum(conv * conv, axis=-1)])
-    sums = lax.psum(sums, cols + ("tp",))
+    sums = sum_small(cols, sizes, sums.reshape((-1, 128))).reshape(sums.shape)
     mean_c = (sums[0] / channels)[..., None]
     var_c = (sums[1] / channels)[..., None] - mean_c * mean_c
     gain = lax.dynamic_slice_in_dim(channel_norm_gain, chan_start, chan, 0)
@@ -246,11 +507,7 @@
     attn_out = attn_out.reshape((count * rows, wide))
     mixer = jnp.concatenate([attn_out, conv_out.reshape((count * rows, chan))], axis=1)
     gathered_out = lax.all_gather(out_rows, "sp", axis=1, tiled=True)
-    term = jnp.dot(mixer, gathered_out, preferred_element_type=jnp.float32).astype(jnp.bfloat16)
-    half = term.shape[1] // lax.axis_size("tp")
-    term = jnp.swapaxes(term.reshape((count, rows, -1, half)), 1, 2).reshape((-1, rows, half))
-    mixed = lax.psum_scatter(term, cols + ("tp",), scatter_dimension=0, tiled=True)
-    return mixed
+    return project_out(cols, sizes, rows, mixer, gathered_out)[None]
 
 
 def split_axes(mesh, heads_tp, chan_tp):

time: 268 us -> 180 us (0.67); the launches traced: 264 us -> 179 us
  Pallas kernels: 17.1 us -> 112 us
  waiting for transfers between devices: 107 us -> 14.4 us
  local copies, waits for them, and re-layouts: 47.8 us -> 17 us
  matrix products: 29.8 us -> 1.83 us
  blocking collectives: 22 us -> 0 us
  starting transfers between devices: 18 us -> 14.1 us
    pallas_call x0 -> x3, Pallas kernels: none -> 94.5 us  [the longest x1 59 us: gather_project(): pl.pallas_call(functools.partial(gather_kernel, cols, sizes, ring), out_s...]
    reduce_scatter x1 -> x0, waiting for transfers between devices: 50.8 us -> none  [on_device(): lax.psum_scatter(term, cols + ('tp',), scatter_dimension=0, tiled=True)]
    all_gather x2 -> x0, waiting for transfers between devices: 49.1 us -> none  [the longest x1 34.6 us: on_device(): gathered_in = lax.all_gather(stacked, 'sp', axis=0, tiled=True)]
    dot_general x3 -> x0, matrix products: 24.1 us -> none  [the longest x1 18.4 us: on_device(): jnp.dot(normed, gathered_in, preferred_element_type=jnp.float32)]
    psum x1 -> x0, blocking collectives: 13.1 us -> none  [on_device(): sums = lax.psum(sums, cols + ('tp',))]
    convert_element_type x1 -> x0, local copies, waits for them, and re-layouts: 9.77 us -> none  [on_device(): token_f = token_all.astype(jnp.float32)]
    unnamed x27 -> x28, local copies, waits for them, and re-layouts: 16 us -> 6.84 us
    all_gather x1 -> x0, blocking collectives: 8.9 us -> none  [on_device(): spikes = lax.all_gather(spikes, cols, axis=0, tiled=False)]
  transfers between devices with their start and end apart: 9 -> 5, of which waited for: 5 -> 2; matrix products, arithmetic and copies ran while one was open for 25% -> 8% of each run, Pallas kernels for 6% -> 13%
where the time goes in v2:
time: 180 us; the launch traced here: 179 us
  Pallas kernels  112 us (62%)
  local copies, waits for them, and re-layouts  17 us (9%)
  between operations  14.5 us (8%)
  waiting for transfers between devices  14.4 us (8%)
  starting transfers between devices  14.1 us (8%)
  other arithmetic  5.28 us (3%)
  matrix products  1.83 us (1%)
    pallas_call x1, Pallas kernels, gather_project(): pl.pallas_call(functools.partial(gather_kernel, cols, sizes, ring), out_s...  59 us
    pallas_call x1, Pallas kernels, project_out(): pl.pallas_call(functools.partial(project_kernel, cols, sizes), out_shape=...  29.4 us
    pallas_call x1, Pallas kernels, delta_terms(): pl.pallas_call(delta_kernel, grid=(units // group,), out_shape=(jax.Shape...  17.1 us
    ppermute x4, waiting for transfers between devices, from_behind(): return lax.ppermute(block, axis, route)  14.3 us
    ppermute x4, starting transfers between devices, from_behind(): return lax.ppermute(block, axis, route)  14.1 us
    unnamed x28, local copies, waits for them, and re-layouts  6.84 us
    pallas_call x1, Pallas kernels, sum_small(): pl.pallas_call(functools.partial(sum_kernel, cols, sizes), out_shape=jax....  6.01 us
  transfers between devices with their start and end apart: 5, of which 2 were waited for; matrix products, arithmetic and copies ran while one was open for 8% of the time, Pallas kernels for 13%

profile of v2, /device:TPU:0, one launch (start us, length us, event | category | flops | bytes accessed | tf_op | source)
XLA Modules:
  0.0 178.6 jit_solution(16707252931000660371)
XLA Ops:
  6.5 0.7 reshape.103.spike_ref
  7.2 0.8 constant_dynamic-slice_fusion.4
  8.1 0.3 copy.31
  8.4 1.0 dynamic-slice_dynamic-update-slice_fusion.4
  9.4 0.9 dynamic-slice_dynamic-update-slice_fusion.3
  10.4 0.9 dynamic-slice_dynamic-update-slice_fusion.2
  11.3 0.9 dynamic-slice_dynamic-update-slice_fusion.1
  12.3 0.9 dynamic-slice_dynamic-update-slice_fusion.w_ref
  13.2 0.1 pad.4.gates_ref
  13.3 59.0 %gather_project.1 = (bf16[1024,640]{1,0:T(8,128)(2,1)S(1)}, f32[1024,128]{1,0:T(8,128)S(1)}, f32[4,8,128]{2,1,0:T(8,128)S(1)}, f32[4,128,128]{2,1,0:T(8,128)S(1)}) custom-call(bf16[256,1024]{1,0:T(8,128)(2,1)S(1)} %bitcast.92, bf16[512,640]{1,0:T(8,128)(2,1)S(1)} %dynamic-slice_dynamic-update-slice_fusion.w_ref, f32[8,128]{1,0:T(8,128)S(1)} %reshape.103.spike_ref, ...), custom_call_target="tpu_custom_call" | custom-call | tf_op jit(solution)/shard_map/gather_project/pallas_call | solution.py:199
  72.4 0.1 multiply_convert_fusion.1
  72.6 2.7 %collective-permute-start.3 = (bf16[4,30,128]{2,1,0:T(8,128)(2,1)S(1)}, bf16[4,30,128]{2,1,0:T(8,128)(2,1)S(1)}, u32[]{:S(2)}, u32[]{:S(2)}) collective-permute-start(bf16[4,30,128]{2,1,0:T(8,128)(2,1)S(1)} %slice.298), channel_id=1, source_target_pairs={{0,4},{4,8},{8,12},{1,5},{5,9},{9,13},{2,6},{6,10},{10,14},{3,7},{... | collective-permute-start | bytes 92168 | tf_op jit(solution)/shard_map/ppermute | solution.py:18
  75.3 0.8 fusion.56
  76.2 0.7 dynamic_slice.51
  76.9 0.2 copy.33
  77.2 0.6 dynamic_slice.49
  78.5 1.2 fusion.36
  79.7 0.3 fusion.41
  80.0 0.1 dot_general.18.cum_row_ref
  80.0 0.2 copy.36.cum_col_ref
  80.3 0.9 copy-done.3
  81.2 17.1 %shard_map.172 = (f32[4,256,128]{2,1,0:T(8,128)S(1)}, f32[4,256,128]{2,1,0:T(8,128)S(1)}, f32[4,128,128]{2,1,0:T(8,128)S(1)}, f32[4,128,128]{2,1,0:T(8,128)S(1)}) custom-call(bf16[4,256,128]{2,1,0:T(8,128)(2,1)S(1)} %bitcast.96, bf16[4,256,128]{2,1,0:T(8,128)(2,1)S(1)} %bitcast.95, bf16[4,256,128]{2,1,0:T(8,128)(2,1)S(1)} %bitcast.94, ...), custom_call_target="tpu_custom_call" | custom-call | flops 12079595520 | bytes 2097152 | tf_op jit(solution)/shard_map/pallas_call | solution.py:370
  98.3 0.4 convolution_add_fusion.3
  98.7 3.6 %collective-permute-start = (f32[4,128,128]{2,1,0:T(8,128)S(1)}, f32[4,128,128]{2,1,0:T(8,128)S(1)}, u32[]{:S(2)}, u32[]{:S(2)}) collective-permute-start(f32[4,128,128]{2,1,0:T(8,128)S(1)} %convolution_add_fusion.3), channel_id=1, source_target_pairs={{0,4},{4,8},{8,12},{1,5},{5,9},{9,13},{2,6},{6,10},{10,14},{3,7},{... | collective-permute-start | bytes 786440 | tf_op jit(solution)/shard_map/ppermute | solution.py:18
  102.3 1.0 constant_dynamic-slice_fusion.1
  103.3 0.7 pad_maximum_fusion.1
  104.0 0.0 all-gather.2.cloned.1.call-update
  104.1 1.2 fusion.50
  105.3 1.1 dynamic-slice_bitcast_fusion.29
  106.3 0.8 dynamic_slice.53
  107.1 0.1 maximum_convert_fusion
  107.2 2.4 %fusion.54 = (f32[4,256]{1,0:T(4,128)S(1)}, f32[4,256]{1,0:T(4,128)S(1)}, f32[4,256,128]{2,1,0:T(8,128)S(1)}) fusion(f32[4,286,128]{2,1,0:T(8,128)S(1)} %maximum_convert_fusion, f32[128]{0:T(128)S(1)} %get-tuple-element.59, f32[128]{0:T(128)S(1)} %get-tuple-element.30, f32[128]{0:T(128)S(1)} %get-tuple-element.31, f32[128]{0:T(128)S(1)} %get-tuple-element.32, ...), kind=kLoop, calls=%fused_computation.150 | loop fusion | flops 8386560 | bytes 16801280 | tf_op jit(solution)/shard_map/reduce_sum | solution.py:495
  109.6 0.6 reshape.109.x_ref
  110.2 6.0 %sum_small.1 = f32[16,128]{1,0:T(8,128)} custom-call(f32[16,128]{1,0:T(8,128)} %reshape.109.x_ref), custom_call_target="tpu_custom_call" | custom-call | tf_op jit(solution)/shard_map/sum_small/pallas_call | solution.py:245
  116.2 0.4 convolution_add_fusion.2
  116.6 2.8 %collective-permute-start.1 = (f32[4,128,128]{2,1,0:T(8,128)S(1)}, f32[4,128,128]{2,1,0:T(8,128)S(1)}, u32[]{:S(2)}, u32[]{:S(2)}) collective-permute-start(f32[4,128,128]{2,1,0:T(8,128)S(1)} %convolution_add_fusion.2), channel_id=1, source_target_pairs={{0,4},{4,8},{8,12},{1,5},{5,9},{9,13},{2,6},{6,10},{10,14},{3,7},{... | collective-permute-start | bytes 786440 | tf_op jit(solution)/shard_map/ppermute | solution.py:18
  119.5 12.0 %collective-permute-done.1 = f32[4,128,128]{2,1,0:T(8,128)S(1)} collective-permute-done((f32[4,128,128]{2,1,0:T(8,128)S(1)}, f32[4,128,128]{2,1,0:T(8,128)S(1)}, u32[]{:S(2)}, u32[]{:S(2)}) %collective-permute-start.1) | collective-permute-done | bytes 262176 | tf_op jit(solution)/shard_map/ppermute | solution.py:18
  131.5 0.4 convolution_add_fusion.1
  131.9 5.0 %collective-permute-start.2 = (bf16[4,128,128]{2,1,0:T(8,128)(2,1)S(1)}, bf16[4,128,128]{2,1,0:T(8,128)(2,1)S(1)}, u32[]{:S(2)}, u32[]{:S(2)}) collective-permute-start(bf16[4,128,128]{2,1,0:T(8,128)(2,1)S(1)} %convolution_add_fusion.1), channel_id=1, source_target_pairs={{0,4},{4,8},{8,12},{1,5},{5,9},{9,13},{2,6},{6,10},{10,14},{3,7},{... | collective-permute-start | bytes 393224 | tf_op jit(solution)/shard_map/ppermute | solution.py:18
  136.9 0.4 multiply_convert_fusion
  137.3 2.4 %collective-permute-done.2 = bf16[4,128,128]{2,1,0:T(8,128)(2,1)S(1)} collective-permute-done((bf16[4,128,128]{2,1,0:T(8,128)(2,1)S(1)}, bf16[4,128,128]{2,1,0:T(8,128)(2,1)S(1)}, u32[]{:S(2)}, u32[]{:S(2)}) %collective-permute-start.2) | collective-permute-done | bytes 131104 | tf_op jit(solution)/shard_map/ppermute | solution.py:18
  139.6 0.4 multiply_reduce_fusion.1
  140.0 0.2 multiply_convert_fusion.2
  140.2 0.1 pad_maximum_fusion.mix_ref
  140.3 0.0 all-gather.2.cloned.1.call-done.w_ref
  140.3 1.2 copy-done
  141.5 29.4 %project_out.1 = bf16[256,1024]{1,0:T(8,128)(2,1)S(1)} custom-call(bf16[1024,256]{1,0:T(8,128)(2,1)S(1)} %pad_maximum_fusion.mix_ref, bf16[256,2048]{1,0:T(8,128)(2,1)S(1)} %copy-done), custom_call_target="tpu_custom_call" | custom-call | tf_op jit(solution)/shard_map/project_out/pallas_call | solution.py:305
  171.0 0.8 copy.45
  (36 shorter events, 0.2 us)
Async XLA Ops:
  6.5 133.8 %all-gather.2.cloned.1.call-start = ((), (), s32[]{:S(2)}) async-start(), calls=%async_computation | async-start | bytes 1310720 | tf_op jit(solution)/shard_map/all_gather | solution.py:509
  8.4 4.9 %copy-start.1 = (bf16[1,256,1024]{2,1,0:T(8,128)(2,1)S(1)}, bf16[1,256,1024]{2,1,0:T(8,128)(2,1)}, u32[]{:S(2)}) copy-start(bf16[1,256,1024]{2,1,0:T(8,128)(2,1)} %param.18) | copy-start | bytes 1572868
  8.4 4.9 %copy-start.2 = (f32[1,4,128,128]{3,2,1,0:T(8,128)S(1)}, f32[1,4,128,128]{3,2,1,0:T(8,128)}, u32[]{:S(2)}) copy-start(f32[1,4,128,128]{3,2,1,0:T(8,128)} %param.30) | copy-start | bytes 786436
  8.4 4.9 %copy-start.4 = (f32[2048]{0:T(1024)S(1)}, f32[2048]{0:T(1024)}, u32[]{:S(2)}) copy-start(f32[2048]{0:T(1024)} %param.19) | copy-start | bytes 24580
  72.5 3.7 %copy-start.5 = (bf16[1024,128]{1,0:T(8,128)(2,1)}, bf16[1024,128]{1,0:T(8,128)(2,1)S(1)}, u32[]{:S(2)}) copy-start(bf16[1024,128]{1,0:T(8,128)(2,1)S(1)} %multiply_convert_fusion.1) | copy-start | bytes 786436
  72.6 3.7 %copy-start.9 = (f32[8]{0:T(128)S(1)}, f32[8]{0:T(128)}, u32[]{:S(2)}) copy-start(f32[8]{0:T(128)} %param.28) | copy-start | bytes 100
  72.6 34.5 %collective-permute-start.3 = (bf16[4,30,128]{2,1,0:T(8,128)(2,1)S(1)}, bf16[4,30,128]{2,1,0:T(8,128)(2,1)S(1)}, u32[]{:S(2)}, u32[]{:S(2)}) collective-permute-start(bf16[4,30,128]{2,1,0:T(8,128)(2,1)S(1)} %slice.298), channel_id=1, source_target_pairs={{0,4},{4,8},{8,12},{1,5},{5,9},{9,13},{2,6},{6,10},{10,14},{3,7},{... | collective-permute-start | bytes 92168 | tf_op jit(solution)/shard_map/ppermute | solution.py:18
  76.1 1.0 copy-start.10
  80.3 1.0 copy-start.3
  98.3 8.8 %copy-start.6 = (bf16[1024,128]{1,0:T(8,128)(2,1)S(1)}, bf16[1024,128]{1,0:T(8,128)(2,1)}, u32[]{:S(2)}) copy-start(bf16[1024,128]{1,0:T(8,128)(2,1)} %copy-done.5) | copy-start | bytes 786436
  98.7 17.5 %collective-permute-start = (f32[4,128,128]{2,1,0:T(8,128)S(1)}, f32[4,128,128]{2,1,0:T(8,128)S(1)}, u32[]{:S(2)}, u32[]{:S(2)}) collective-permute-start(f32[4,128,128]{2,1,0:T(8,128)S(1)} %convolution_add_fusion.3), channel_id=1, source_target_pairs={{0,4},{4,8},{8,12},{1,5},{5,9},{9,13},{2,6},{6,10},{10,14},{3,7},{... | collective-permute-start | bytes 786440 | tf_op jit(solution)/shard_map/ppermute | solution.py:18
  116.2 3.3 %copy-start.7 = (f32[16,128]{1,0:T(8,128)S(1)}, f32[16,128]{1,0:T(8,128)}, u32[]{:S(2)}) copy-start(f32[16,128]{1,0:T(8,128)} %sum_small.1) | copy-start | bytes 24580
  116.6 14.9 %collective-permute-start.1 = (f32[4,128,128]{2,1,0:T(8,128)S(1)}, f32[4,128,128]{2,1,0:T(8,128)S(1)}, u32[]{:S(2)}, u32[]{:S(2)}) collective-permute-start(f32[4,128,128]{2,1,0:T(8,128)S(1)} %convolution_add_fusion.2), channel_id=1, source_target_pairs={{0,4},{4,8},{8,12},{1,5},{5,9},{9,13},{2,6},{6,10},{10,14},{3,7},{... | collective-permute-start | bytes 786440 | tf_op jit(solution)/shard_map/ppermute | solution.py:18
  131.9 7.7 %collective-permute-start.2 = (bf16[4,128,128]{2,1,0:T(8,128)(2,1)S(1)}, bf16[4,128,128]{2,1,0:T(8,128)(2,1)S(1)}, u32[]{:S(2)}, u32[]{:S(2)}) collective-permute-start(bf16[4,128,128]{2,1,0:T(8,128)(2,1)S(1)} %convolution_add_fusion.1), channel_id=1, source_target_pairs={{0,4},{4,8},{8,12},{1,5},{5,9},{9,13},{2,6},{6,10},{10,14},{3,7},{... | collective-permute-start | bytes 393224 | tf_op jit(solution)/shard_map/ppermute | solution.py:18
  136.9 3.1 %copy-start.8 = (f32[128]{0:T(128)S(1)}, f32[128]{0:T(128)}, u32[]{:S(2)}) copy-start(f32[128]{0:T(128)} %param.31) | copy-start | bytes 1540
  140.3 1.2 copy-start
Sparse Core Ops, SparseCore 0:
  104.2 28.9 all-gather.1
